TPU v7x, 128 devices: a whole 4x4x4 slice. The times are simulated.
128 devices in a mesh: sp: 16 (over z, x), tp: 8 (over y, core).
Axes of the slice: x: 4, y: 4, z: 4, core: 2. Of those that a mesh axis runs over, the one named last changes fastest.
Arguments:
- latent: bfloat16 [8192, 4096], P('sp'), may hold values from -64 to 64
- context: bfloat16 [1024, 4096], P('sp'), may hold values from -6 to 6
- condition: bfloat16 [4096], P('sp'), may hold values from -6 to 6
- context_condition: bfloat16 [4096], P('sp'), may hold values from -6 to 6
- shift_weight: bfloat16 [4096, 4096], P('sp', 'tp'), may hold values from -0.125 to 0.125
- scale_weight: bfloat16 [4096, 4096], P('sp', 'tp'), may hold values from -0.125 to 0.125
- gate_weight: bfloat16 [4096, 4096], P('sp', 'tp'), may hold values from -0.25 to 0.25
- norm_gain: float32 [4096], replicated, may hold values from 0.1 to 1.9
- query_weight: bfloat16 [4096, 2048], P(None, 'tp'), may hold values from -0.09375 to 0.09375
- key_weight: bfloat16 [4096, 2048], P(None, 'tp'), may hold values from -0.09375 to 0.09375
- value_weight: bfloat16 [4096, 2048], P(None, 'tp'), may hold values from -0.09375 to 0.09375
- write_weight: bfloat16 [4096, 2, 16], replicated, may hold values from -0.09375 to 0.09375
- decay_weight: bfloat16 [4096, 2, 16], replicated, may hold values from -0.09375 to 0.09375
- write_bias: float32 [2, 16], replicated, may hold values from -12 to 1
- decay_bias: float32 [2, 16], replicated, may hold values from -16 to -4
- log_rate: float32 [2, 16], replicated, may hold values from 0 to 1.4
- head_gain: float32 [128], replicated, may hold values from 0.1 to 1.9
- out_weight: bfloat16 [2048, 4096], P(None, 'tp'), may hold values from -0.125 to 0.125
Outputs:
- updated: bfloat16 [8192, 4096], P('sp', 'tp')
All inputs are finite; a program needn't handle non-finite values.
Results may differ from a plain program's by a relative error of at most 0.013.
Values may be sent and summed in bfloat16 or wider, within the bound.
A program may use at most 128 MiB of HBM per device.

v0:
```python
import jax
import jax.numpy as jnp
from jax import lax
from jax.experimental import pallas as pl
from jax.experimental.pallas import tpu as pltpu
from jax.sharding import Mesh
from jax.sharding import PartitionSpec as P

HEAD_DIM = 128
SP = ("sp_0", "sp_1")
EPS = 0.0001
F32 = jnp.float32
BF16 = jnp.bfloat16
TILE = 128
LEVELS = (1, 2, 3, 4, 5, 6)


def mm(a, b):
    return jnp.dot(a.astype(BF16), b.astype(BF16), preferred_element_type=F32)


def mm_nt(a, b):
    return lax.dot_general(a, b, (((1,), (1,)), ((), ())), preferred_element_type=F32)


def mm_tn(a, b):
    return lax.dot_general(a, b, (((0,), (0,)), ((), ())), preferred_element_type=F32)


def iota2(shape, dim):
    return lax.broadcasted_iota(jnp.int32, shape, dim)


def softplus(u):
    return jnp.maximum(u, 0.0) + jnp.log1p(jnp.exp(-jnp.abs(u)))


def inv_norm(rows_bf16):
    r = rows_bf16.astype(F32)
    return lax.rsqrt(jnp.sum(r * r, axis=-1, keepdims=True) + EPS)


def modulate_rows(lat_ref, ctx_ref, gain_ref, rows_ref, ab_ref, mod_ref):
    for s in range(2):
        ab_ref[2 * s] = gain_ref[...] * (1.0 + rows_ref[2 + s : 3 + s, :])
        ab_ref[2 * s + 1] = rows_ref[s : s + 1, :]
    n_lat = lat_ref.shape[0] // 16
    n_ctx = ctx_ref.shape[0] // 16

    def one(src_ref, base, s):
        def step(i, carry):
            x = src_ref[pl.ds(i * 16, 16), :].astype(F32)
            inv = lax.rsqrt(jnp.mean(x * x, axis=-1, keepdims=True) + EPS)
            y = x * inv * ab_ref[2 * s] + ab_ref[2 * s + 1]
            mod_ref[pl.ds(base + i * 16, 16), :] = y.astype(BF16)
            return carry

        return step

    lax.fori_loop(0, n_lat, one(lat_ref, 0, 0), 0)
    lax.fori_loop(0, n_ctx, one(ctx_ref, lat_ref.shape[0], 1), 0)


def gate_rows(first_head, pre_ref, wb_ref, db_ref, lr_ref, rows_ref, n_lat, n_ctx):
    width = n_lat + TILE
    lane = iota2((8, width), 1)
    is_ctx = lane >= n_lat
    pos = jnp.where(is_ctx, lane - n_lat, lane)
    size = jnp.where(is_ctx, n_ctx, n_lat)
    valid = pos < size
    row = iota2((8, width), 0)
    rates = jnp.zeros((8, width), F32)
    logd = jnp.zeros((8, width), F32)
    for c in range(4):
        d, h = c // 2, c % 2
        head = first_head + h
        at = d * 16 + head
        w = pre_ref[pl.ds(at, 1), :] + wb_ref[d, head]
        u = pre_ref[pl.ds(32 + at, 1), :] + db_ref[d, head]
        rate = 1.0 / (1.0 + jnp.exp(-w))
        step = -jnp.exp(jnp.full((1, width), lr_ref[d, head], F32)) * softplus(u)
        rates = jnp.where(row == c, rate, rates)
        logd = jnp.where(row == c, step, logd)
    rates = jnp.where(valid, rates, 0.0)
    logd = jnp.where(valid, logd, 0.0)
    fwd = logd
    bwd = logd
    s = 1
    while s < n_lat:
        fwd = fwd + jnp.where(pos >= s, pltpu.roll(fwd, s, 1), 0.0)
        bwd = bwd + jnp.where(pos + s < size, pltpu.roll(bwd, width - s, 1), 0.0)
        s *= 2
    g = jnp.where(row < 2, fwd, bwd)
    g = jnp.where(valid, g, 0.0)
    whole_lat = jnp.sum(jnp.where(is_ctx, 0.0, logd), axis=1, keepdims=True)
    whole_ctx = jnp.sum(jnp.where(is_ctx, logd, 0.0), axis=1, keepdims=True)
    late = jnp.exp(jnp.where(is_ctx, whole_ctx, whole_lat) - g)
    eg = jnp.exp(g)
    parts = []
    for a in (rates, g, late, eg):
        up = pltpu.roll(pltpu.roll(a, n_ctx, 1), 6, 0)
        a = jnp.where(lane >= n_lat + n_ctx, up, a)
        parts.append(a)
    rows_ref[...] = jnp.zeros_like(rows_ref)
    for n, a in enumerate(parts):
        rows_ref[8 * n : 8 * n + 8, :] = a
    return jnp.exp(whole_lat), jnp.exp(whole_ctx)


def tile_inverse(a_ref, t_ref, index, ones_diag, xor):
    a = a_ref[index].astype(F32)
    t = ones_diag - jnp.where(xor == 1, a, 0.0)
    return a, t


def recurrence(first_head, q_ref, k_ref, v_ref, pre_ref, wb_ref, db_ref, lr_ref, scratch, outs, n_lat, n_ctx):
    rows_ref, cols_ref, gk_ref, qk_ref, ad_ref, t_ref, ao_ref, p_ref, x_ref, xl_ref = scratch
    o1_ref, q2_ref, lat_map_ref, ctx_map_ref = outs
    blocks = n_lat // TILE
    width = n_lat + TILE
    dec_lat, dec_ctx = gate_rows(first_head, pre_ref, wb_ref, db_ref, lr_ref, rows_ref, n_lat, n_ctx)
    for b in range(blocks + 1):
        cols_ref[b * TILE : (b + 1) * TILE, :] = jnp.transpose(rows_ref[:, b * TILE : (b + 1) * TILE])
    RATE, G, LATE, EG = 0, 8, 16, 24

    def kcols(h):
        return k_ref[0:n_lat, h * TILE : (h + 1) * TILE]

    def kctx(h):
        kc = k_ref[n_lat : n_lat + n_ctx, h * TILE : (h + 1) * TILE]
        return jnp.concatenate([kc, kc], axis=0)

    def vctx(h):
        vc = v_ref[n_lat : n_lat + n_ctx, h * TILE : (h + 1) * TILE]
        return jnp.concatenate([vc, vc], axis=0)

    kinv = []
    for h in range(2):
        kinv.append(jnp.concatenate([inv_norm(kcols(h)), inv_norm(kctx(h))], axis=0))
    lane128 = iota2((width, TILE), 1)
    both = jnp.where(lane128 == 0, kinv[0], jnp.where(lane128 == 1, kinv[1], 0.0))
    for b in range(blocks + 1):
        rows_ref[:, b * TILE : (b + 1) * TILE] = jnp.where(
            (iota2((TILE, TILE), 0) < 32),
            rows_ref[:, b * TILE : (b + 1) * TILE],
            pltpu.roll(jnp.transpose(both[b * TILE : (b + 1) * TILE, :]), 32, 0),
        )
    KINV = 32
    ii = iota2((TILE, TILE), 0)
    jj = iota2((TILE, TILE), 1)
    xor = ii ^ jj
    qinvs = []
    for h in range(2):
        qh = q_ref[0:n_lat, h * TILE : (h + 1) * TILE]
        qinv = inv_norm(qh) * (HEAD_DIM**-0.5)
        qinvs.append(qinv)
        krow = rows_ref[KINV + h : KINV + h + 1, 0:n_lat]
        gk_ref[h] = mm_nt(kcols(h), kcols(h)) * kinv[h][0:n_lat] * krow
        qk_ref[h] = mm_nt(qh, kcols(h)) * qinv * krow

    def spread(c, i, j):
        gi = cols_ref[i * TILE : (i + 1) * TILE, G + c : G + c + 1]
        gj = rows_ref[G + c : G + c + 1, j * TILE : (j + 1) * TILE]
        return gi - gj

    for c in range(4):
        d, h = c // 2, c % 2
        for i in range(blocks):
            ri = cols_ref[i * TILE : (i + 1) * TILE, RATE + c : RATE + c + 1]
            for j in range(blocks):
                if (d == 0 and j > i) or (d == 1 and j < i):
                    continue
                at = (slice(i * TILE, (i + 1) * TILE), slice(j * TILE, (j + 1) * TILE))
                sp = spread(c, i, j)
                if i == j:
                    keep = (ii >= jj) if d == 0 else (ii <= jj)
                    dm = jnp.where(keep, jnp.exp(jnp.where(keep, sp, 0.0)), 0.0)
                else:
                    dm = jnp.exp(sp)
                a = gk_ref[(h, *at)] * dm * ri
                if i == j:
                    ad_ref[c * blocks + i] = jnp.where(ii == jj, 0.0, a).astype(BF16)
                else:
                    ao_ref[(c, *at)] = a.astype(BF16)
                p_ref[(c, *at)] = (qk_ref[(h, *at)] * dm).astype(BF16)
    for h in range(2):
        kc = kctx(h)
        g2 = mm_nt(kc, kc) * kinv[h][n_lat:] * rows_ref[KINV + h : KINV + h + 1, n_lat:]
        keep = jnp.where(
            ii < n_ctx, jnp.where(jj < ii, 1, 0), jnp.where(jj > ii, 1, 0)
        )
        keep = jnp.where((ii < n_ctx) == (jj < n_ctx), keep, 0) == 1
        sp = (
            cols_ref[n_lat:, G + h : G + h + 1]
            - rows_ref[G + h : G + h + 1, n_lat:]
        )
        dm = jnp.where(keep, jnp.exp(jnp.where(keep, sp, 0.0)), 0.0)
        ad_ref[4 * blocks + h] = (g2 * dm * cols_ref[n_lat:, RATE + h : RATE + h + 1]).astype(BF16)

    tiles = 4 * blocks + 2
    group = tiles // 2

    def invert(part, carry):
        base = part * group
        eye = jnp.where(xor == 0, 1.0, 0.0)
        ts = []
        for n in range(group):
            a = ad_ref[base + n].astype(F32)
            ts.append((eye - jnp.where(xor == 1, a, 0.0)).astype(BF16))
        for level in LEVELS:
            xs = []
            for n in range(group):
                off = jnp.where((xor >> level) == 1, ad_ref[base + n].astype(F32), 0.0).astype(BF16)
                xs.append(mm(ts[n], off).astype(BF16))
            ts = [(t.astype(F32) - mm(x, t)).astype(BF16) for x, t in zip(xs, ts)]
        for n in range(group):
            t_ref[base + n] = ts[n]
        return carry

    lax.fori_loop(0, 2, invert, 0)

    for c in range(4):
        d, h = c // 2, c % 2
        order = list(range(blocks)) if d == 0 else list(reversed(range(blocks)))
        for n, i in enumerate(order):
            r = slice(i * TILE, (i + 1) * TILE)
            rate = cols_ref[r, RATE + c : RATE + c + 1]
            eg = cols_ref[r, EG + c : EG + c + 1]
            late = cols_ref[r, LATE + c : LATE + c + 1]
            ki = kinv[h][r]
            vi = v_ref[r, h * TILE : (h + 1) * TILE].astype(F32) * rate
            wi = k_ref[r, h * TILE : (h + 1) * TILE].astype(F32) * (rate * eg * ki)
            b = jnp.concatenate([vi, wi], axis=1)
            if n > 0:
                done = slice(0, i * TILE) if d == 0 else slice((i + 1) * TILE, n_lat)
                b = b - mm(ao_ref[c, r, done], x_ref[c, done, :])
            x = mm(t_ref[c * blocks + i], b)
            x_ref[c, r, :] = x.astype(BF16)
            xl_ref[c, r, :] = (x * (late * ki)).astype(BF16)
    for h in range(2):
        o1 = []
        for d in range(2):
            c = d * 2 + h
            for i in range(blocks):
                r = slice(i * TILE, (i + 1) * TILE)
                seen = slice(0, (i + 1) * TILE) if d == 0 else slice(i * TILE, n_lat)
                ow = mm(p_ref[c, r, seen], x_ref[c, seen, :])
                qi = q_ref[r, h * TILE : (h + 1) * TILE].astype(F32)
                early = qi * (cols_ref[r, EG + c : EG + c + 1] * qinvs[h][r])
                q2_ref[h, r, d * TILE : (d + 1) * TILE] = (early - ow[:, TILE:]).astype(BF16)
                if d == 0:
                    o1.append(ow[:, :TILE])
                else:
                    o1_ref[h, r, :] = o1[i] + ow[:, :TILE]
            m = mm_tn(kcols(h), xl_ref[c])
            diag = jnp.where(xor == 0, dec_lat[c : c + 1, :], 0.0)
            lat_map_ref[c] = jnp.concatenate([diag - m[:, TILE:], m[:, :TILE]], axis=1).astype(BF16)
    for h in range(2):
        ci = kinv[h][n_lat:]
        cr = slice(n_lat, n_lat + TILE)
        rate = cols_ref[cr, RATE + h : RATE + h + 1]
        eg = cols_ref[cr, EG + h : EG + h + 1]
        late = cols_ref[cr, LATE + h : LATE + h + 1]
        kc = kctx(h)
        b = jnp.concatenate([vctx(h).astype(F32) * rate, kc.astype(F32) * (rate * eg * ci)], axis=1)
        x = mm(t_ref[4 * blocks + h], b)
        xl = (x * (late * ci)).astype(BF16)
        for d in range(2):
            c = d * 2 + h
            m = mm_tn(kc[0:n_ctx], xl[d * n_ctx : (d + 1) * n_ctx])
            diag = jnp.where(xor == 0, dec_ctx[c : c + 1, :], 0.0)
            ctx_map_ref[c] = jnp.concatenate([diag - m[:, TILE:], m[:, :TILE]], axis=1).astype(BF16)


def make_local_kernel(first_head_of):
    def kernel(
        lat_ref, ctx_ref, rows_in, gain_ref, wq_hbm, wk_hbm, wv_hbm, ww_ref, wd_ref, wb_ref, db_ref, lr_ref,
        o1_ref, q2_ref, lat_map_ref, ctx_map_ref,
        w_ref, sem, ab_ref, mod_ref, q_ref, k_ref, v_ref, pre_ref, *scratch,
    ):
        n_lat, n_ctx = lat_ref.shape[0], ctx_ref.shape[0]
        copies = [
            pltpu.make_async_copy(src, w_ref.at[n], sem.at[n])
            for n, src in enumerate((wk_hbm, wv_hbm, wq_hbm))
        ]
        for copy in copies:
            copy.start()
        modulate_rows(lat_ref, ctx_ref, gain_ref, rows_in, ab_ref, mod_ref)
        pre_ref[...] = jnp.zeros_like(pre_ref)
        for n, w in enumerate((ww_ref, wd_ref)):
            r = slice(32 * n, 32 * n + 32)
            pre_ref[r, 0:n_lat] = mm_nt(w[...], mod_ref[0:n_lat, :]).astype(BF16).astype(F32)
            pre_ref[r, n_lat : n_lat + n_ctx] = mm_nt(w[...], mod_ref[n_lat:, :]).astype(BF16).astype(F32)
        copies[0].wait()
        k_ref[...] = mm(mod_ref[...], w_ref[0]).astype(BF16)
        copies[1].wait()
        v_ref[...] = mm(mod_ref[...], w_ref[1]).astype(BF16)
        copies[2].wait()
        q_ref[...] = mm(mod_ref[0:n_lat, :], w_ref[2]).astype(BF16)
        recurrence(
            first_head_of(), q_ref, k_ref, v_ref, pre_ref, wb_ref, db_ref, lr_ref, scratch,
            (o1_ref, q2_ref, lat_map_ref, ctx_map_ref), n_lat, n_ctx,
        )

    return kernel


def local_scratch(n_lat, n_ctx, width):
    blocks = n_lat // TILE
    tiles = 4 * blocks + 2
    return [
        pltpu.VMEM((3, width, 2 * TILE), BF16),
        pltpu.SemaphoreType.DMA((3,)),
        pltpu.VMEM((4, 1, width), F32),
        pltpu.VMEM((n_lat + n_ctx, width), BF16),
        pltpu.VMEM((n_lat, 2 * TILE), BF16),
        pltpu.VMEM((n_lat + n_ctx, 2 * TILE), BF16),
        pltpu.VMEM((n_lat + n_ctx, 2 * TILE), BF16),
        pltpu.VMEM((64, n_lat + TILE), F32),
        pltpu.VMEM((TILE, n_lat + TILE), F32),
        pltpu.VMEM((n_lat + TILE, TILE), F32),
        pltpu.VMEM((2, n_lat, n_lat), F32),
        pltpu.VMEM((2, n_lat, n_lat), F32),
        pltpu.VMEM((tiles, TILE, TILE), BF16),
        pltpu.VMEM((tiles, TILE, TILE), BF16),
        pltpu.VMEM((4, n_lat, n_lat), BF16),
        pltpu.VMEM((4, n_lat, n_lat), BF16),
        pltpu.VMEM((4, n_lat, 2 * TILE), BF16),
        pltpu.VMEM((4, n_lat, 2 * TILE), BF16),
    ]


def local_call(first_head_of, args):
    latent, context = args[0], args[1]
    n_lat, width = latent.shape
    n_ctx = context.shape[0]
    vm = pl.BlockSpec(memory_space=pltpu.VMEM)
    sm = pl.BlockSpec(memory_space=pltpu.SMEM)
    hb = pl.BlockSpec(memory_space=pl.ANY)
    return pl.pallas_call(
        make_local_kernel(first_head_of),
        out_shape=(
            jax.ShapeDtypeStruct((2, n_lat, TILE), F32),
            jax.ShapeDtypeStruct((2, n_lat, 2 * TILE), BF16),
            jax.ShapeDtypeStruct((4, TILE, 2 * TILE), BF16),
            jax.ShapeDtypeStruct((4, TILE, 2 * TILE), BF16),
        ),
        in_specs=[vm, vm, vm, vm, hb, hb, hb, vm, vm, sm, sm, sm],
        out_specs=(vm, vm, vm, vm),
        scratch_shapes=local_scratch(n_lat, n_ctx, width),
        compiler_params=pltpu.CompilerParams(vmem_limit_bytes=60 * 1024 * 1024),
        name="local_tokens",
    )(*args)


def split_rows(x):
    hi = x.astype(BF16)
    lo = (x - hi.astype(F32)).astype(BF16)
    return hi, lo


def mul_precise(m_bf16, x):
    hi, lo = split_rows(x)
    n = x.shape[1]
    y = jnp.dot(m_bf16, jnp.concatenate([hi, lo], axis=1), preferred_element_type=F32)
    return y[:, :n] + y[:, n:]


def then(next_map, total):
    y = mul_precise(next_map[:, :TILE], total)
    zero = jnp.zeros((TILE, TILE), F32)
    return y + jnp.concatenate([zero, next_map[:, TILE:].astype(F32)], axis=1)


def row_scan_kernel(x_of):
    def kernel(maps_ref, prefix_ref, total_ref):
        backwards = x_of() >= 2
        peers = maps_ref.shape[0]
        for part in range(2):
            total = None
            for n in range(peers):
                at = jnp.where(backwards, peers - 1 - n, n)
                one = maps_ref[at, part]
                if part == 1:
                    if n == 0:
                        eye = jnp.where(iota2((TILE, 2 * TILE), 0) == iota2((TILE, 2 * TILE), 1), 1.0, 0.0)
                        prefix_ref[at] = eye
                    else:
                        prefix_ref[at] = total
                total = one.astype(F32) if n == 0 else then(one, total)
            total_ref[part] = total.astype(BF16)

    return kernel


def column_scan_kernel(x_of, z_of):
    def kernel(totals_ref, prefix_ref, start_ref):
        backwards = x_of() >= 2
        groups = totals_ref.shape[0]
        state = None
        for n in range(groups):
            at = jnp.where(backwards, groups - 1 - n, n)
            one = totals_ref[at, 0]
            off = one[:, TILE:].astype(F32)
            state = off if n == 0 else mul_precise(one[:, :TILE], state) + off
        z = z_of()
        place = jnp.where(backwards, groups - 1 - z, z)
        for n in range(groups - 1):
            at = jnp.where(backwards, groups - 1 - n, n)
            one = totals_ref[at, 1]
            new = mul_precise(one[:, :TILE], state) + one[:, TILE:].astype(F32)
            state = jnp.where(n < place, new, state)
        for k in range(prefix_ref.shape[0]):
            mk = prefix_ref[k]
            hi, lo = split_rows(mk[:, :TILE])
            s = mul_precise(hi, state) + mm(lo, state) + mk[:, TILE:]
            start_ref[k] = s.astype(BF16)

    return kernel


def apply_kernel(o1_ref, q2_ref, s_ref, gain_ref, out_ref):
    for h in range(2):
        both = jnp.concatenate([s_ref[h], s_ref[2 + h]], axis=0)
        y = o1_ref[h] + jnp.dot(q2_ref[h], both, preferred_element_type=F32)
        y = y * lax.rsqrt(jnp.mean(y * y, axis=-1, keepdims=True) + EPS) * gain_ref[...]
        out_ref[:, h * TILE : (h + 1) * TILE] = y.astype(BF16)


def body(
    latent, context, condition, context_condition, shift_weight, scale_weight, gate_weight, norm_gain,
    query_weight, key_weight, value_weight, write_weight, decay_weight, write_bias, decay_bias, log_rate,
    head_gain, out_weight,
):
    own_cols = gate_weight.shape[1]
    col_start = lax.axis_index("tp") * own_cols
    stacked = jnp.stack([condition, context_condition]).astype(F32)
    silu_rows = jax.nn.silu(stacked).astype(BF16)
    part = jnp.concatenate(
        [
            jnp.dot(silu_rows, shift_weight, preferred_element_type=F32),
            jnp.dot(silu_rows, scale_weight, preferred_element_type=F32),
            jnp.dot(silu_rows[:1], gate_weight, preferred_element_type=F32),
        ],
        axis=0,
    )
    copies = jnp.broadcast_to(part, (16, *part.shape))
    summed = jnp.sum(lax.all_to_all(copies, SP, split_axis=0, concat_axis=0, tiled=True), axis=0)
    gate_row = summed[4:5]
    mod_rows = lax.all_gather(summed[:4], "tp", axis=1, tiled=True)
    gates = [jnp.transpose(w, (1, 2, 0)).reshape(32, -1) for w in (write_weight, decay_weight)]
    o1, q2, lat_map, ctx_map = local_call(
        lambda: lax.axis_index("tp") * 2,
        (
            latent, context, mod_rows, norm_gain.reshape(1, -1), query_weight, key_weight, value_weight,
            *gates, write_bias, decay_bias, log_rate,
        ),
    )
    vm = pl.BlockSpec(memory_space=pltpu.VMEM)
    maps = lax.all_to_all(
        jnp.stack([ctx_map, lat_map], axis=1), "sp_1", split_axis=0, concat_axis=0, tiled=True
    )
    prefix, totals = pl.pallas_call(
        row_scan_kernel(lambda: lax.axis_index("sp_1")),
        out_shape=(
            jax.ShapeDtypeStruct((4, TILE, 2 * TILE), F32),
            jax.ShapeDtypeStruct((2, TILE, 2 * TILE), BF16),
        ),
        in_specs=[vm], out_specs=(vm, vm), name="row_scan",
    )(maps)
    all_totals = lax.all_gather(totals, "sp_0", axis=0)
    starts = pl.pallas_call(
        column_scan_kernel(lambda: lax.axis_index("sp_1"), lambda: lax.axis_index("sp_0")),
        out_shape=jax.ShapeDtypeStruct((4, TILE, TILE), BF16),
        in_specs=[vm, vm], out_specs=vm, name="column_scan",
    )(all_totals, prefix)
    mine = lax.all_to_all(starts, "sp_1", split_axis=0, concat_axis=0, tiled=True)
    head_out = pl.pallas_call(
        apply_kernel,
        out_shape=jax.ShapeDtypeStruct((latent.shape[0], 2 * TILE), BF16),
        in_specs=[vm] * 4, out_specs=vm, name="apply_start",
    )(o1, q2, mine, head_gain.reshape(1, -1))
    branch = jnp.dot(
        lax.all_gather(head_out, "tp", axis=1, tiled=True), out_weight, preferred_element_type=F32
    )
    residual = lax.dynamic_slice_in_dim(latent, col_start, own_cols, 1).astype(F32)
    return (residual + gate_row * branch).astype(BF16)


def solution(mesh):
    torus = Mesh(mesh.devices.reshape(4, 4, mesh.shape["tp"]), ("sp_0", "sp_1", "tp"))
    placed = (
        P(SP, None), P(SP, None), P(SP), P(SP), P(SP, "tp"), P(SP, "tp"), P(SP, "tp"), P(),
        P(None, "tp"), P(None, "tp"), P(None, "tp"), P(), P(), P(), P(), P(), P(), P(None, "tp"),
    )
    return jax.shard_map(body, mesh=torus, in_specs=placed, out_specs=P(SP, "tp"), check_vma=False)
```

profile of v0, /device:TPU:1, one launch (start us, length us, event | category | flops | bytes accessed | tf_op | source)
XLA Modules:
  0.0 153.0 jit_solution(6113486625307302761)
XLA Ops:
  6.5 0.0 copy-start
  6.5 0.0 all-gather.3.cloned.1.call-start
  6.5 0.8 stack.18
  7.3 0.7 stack.19
  8.0 1.1 fusion.5
  9.1 1.1 fusion.7
  10.2 1.1 fusion.6
  11.4 15.8 %all_to_all.15 = f32[16,5,512]{2,1,0:T(8,128)S(1)} all-to-all(f32[16,5,512]{2,1,0:T(8,128)S(1)} %broadcast_in_dim.3), channel_id=1, replica_groups=mesh['sp_0'=4,'sp_1'=4,'tp'=8] {'sp_0','sp_1'}, dimensions={0} | all-to-all | bytes 327680 | tf_op jit(solution)/shard_map/all_to_all | solution.py:448
  27.2 16.3 %all_gather.12.rows_in = f32[4,4096]{1,0:T(4,128)} all-gather(f32[4,512]{1,0:T(4,128)S(1)} %slice.14), channel_id=1, replica_groups=mesh['sp_0'=4,'sp_1'=4,'tp'=8] {'tp'}, dimensions={1}, use_global_device_ids=true | all-gather | bytes 73728 | tf_op jit(solution)/shard_map/all_gather | solution.py:450
  43.5 28.4 %local_tokens.1 = (f32[2,512,128]{2,1,0:T(8,128)}, bf16[2,512,256]{2,1,0:T(8,128)(2,1)}, bf16[4,128,256]{2,1,0:T(8,128)(2,1)}, bf16[4,128,256]{2,1,0:T(8,128)(2,1)}) custom-call(bf16[512,4096]{1,0:T(8,128)(2,1)} %lat_ref.1, bf16[64,4096]{1,0:T(8,128)(2,1)} %ctx_ref.1, f32[4,4096]{1,0:T(4,128)} %all_gather.12.rows_in, f32[1,4096]{1,0:T(1,128)} %bitcast.28, ...), custom_call_target="tpu_custom_call" | custom-call | tf_op jit(solution)/shard_map/local_tokens/pallas_call | solution.py:340
  71.9 1.1 pad_maximum_fusion
  73.0 12.4 %all_to_all.16.maps_ref = bf16[4,2,128,256]{3,2,1,0:T(8,128)(2,1)} all-to-all(bf16[4,2,128,256]{3,2,1,0:T(8,128)(2,1)S(1)} %pad_maximum_fusion), channel_id=1, replica_groups=mesh['sp_0'=4,'sp_1'=4,'tp'=8] {'sp_1'}, dimensions={0} | all-to-all | bytes 1048576 | tf_op jit(solution)/shard_map/all_to_all | solution.py:460
  85.3 2.5 %row_scan.1 = (f32[4,128,256]{2,1,0:T(8,128)}, bf16[2,128,256]{2,1,0:T(8,128)(2,1)}) custom-call(bf16[4,2,128,256]{3,2,1,0:T(8,128)(2,1)} %all_to_all.16.maps_ref), custom_call_target="tpu_custom_call" | custom-call | tf_op jit(solution)/shard_map/row_scan/pallas_call | solution.py:463
  87.9 11.1 %all-gather = bf16[8,128,256]{2,1,0:T(8,128)(2,1)} all-gather(bf16[2,128,256]{2,1,0:T(8,128)(2,1)} %get-tuple-element.15), channel_id=2, replica_groups=mesh['sp_0'=4,'sp_1'=4,'tp'=8] {'sp_0'}, dimensions={0}, use_global_device_ids=true | all-gather | bytes 655360 | tf_op jit(solution)/shard_map/all_gather | solution.py:471
  99.0 3.0 %column_scan.1 = bf16[4,128,128]{2,1,0:T(8,128)(2,1)} custom-call(bf16[4,2,128,256]{3,2,1,0:T(8,128)(2,1)} %bitcast.23, f32[4,128,256]{2,1,0:T(8,128)} %get-tuple-element.16.prefix_ref), custom_call_target="tpu_custom_call" | custom-call | tf_op jit(solution)/shard_map/column_scan/pallas_call | solution.py:472
  102.0 8.8 %all_to_all.17.s_ref = bf16[4,128,128]{2,1,0:T(8,128)(2,1)} all-to-all(bf16[4,128,128]{2,1,0:T(8,128)(2,1)} %column_scan.1), channel_id=1, replica_groups=mesh['sp_0'=4,'sp_1'=4,'tp'=8] {'sp_1'}, dimensions={0} | all-to-all | bytes 262144 | tf_op jit(solution)/shard_map/all_to_all | solution.py:477
  110.9 2.3 %apply_start.1 = bf16[512,256]{1,0:T(8,128)(2,1)} custom-call(f32[2,512,128]{2,1,0:T(8,128)} %get-tuple-element.11.o1_ref, bf16[2,512,256]{2,1,0:T(8,128)(2,1)} %get-tuple-element.12.q2_ref, bf16[4,128,128]{2,1,0:T(8,128)(2,1)} %all_to_all.17.s_ref, f32[1,128]{1,0:T(1,128)} %bitcast.30), custom_call_target="tpu_custom_call" | custom-call | tf_op jit(solution)/shard_map/apply_start/pallas_call | solution.py:478
  113.2 0.0 all-gather.3.cloned.1.call-update
  113.2 29.2 %all-gather.3.cloned.1.call-done = bf16[512,2048]{1,0:T(8,128)(2,1)} async-done(((bf16[512,256]{1,0:T(8,128)(2,1)}), bf16[512,2048]{1,0:T(8,128)(2,1)}) %all-gather.3.cloned.1.call-update) | async-done | bytes 2097168 | tf_op jit(solution)/shard_map/all_gather | solution.py:484
  142.4 0.0 copy-done
  142.4 3.7 %fusion.1 = bf16[512,512]{1,0:T(8,128)(2,1)} fusion(bf16[512,2048]{1,0:T(8,128)(2,1)} %all-gather.3.cloned.1.call-done, bf16[2048,512]{1,0:T(8,128)(2,1)S(1)} %copy-done, f32[512]{0:T(512)S(1)} %bitcast.29, bf16[512,4096]{1,0:T(8,128)(2,1)} %lat_ref.1, s32[]{:T(128)S(6)} %select_n.3), kind=kOutput, calls=%fused_computation.2 | convolution fusion | flops 1074790400 | bytes 5244932 | tf_op jit(solution)/shard_map/dot_general | solution.py:483
  (6 shorter events, 0.1 us)
Async XLA Ops:
  6.5 135.9 %copy-start = (bf16[2048,512]{1,0:T(8,128)(2,1)S(1)}, bf16[2048,512]{1,0:T(8,128)(2,1)}, u32[]{:S(2)}) copy-start(bf16[2048,512]{1,0:T(8,128)(2,1)} %param.35) | copy-start | bytes 6291460
  6.5 135.9 %all-gather.3.cloned.1.call-start = ((), (), s32[]{:S(2)}) async-start(), calls=%async_computation.3 | async-start | bytes 2359296 | tf_op jit(solution)/shard_map/all_gather | solution.py:484
Sparse Core Ops, SparseCore 0:
  113.3 29.0 all-gather.2
where the time goes:
time: 154 us; the launch traced here: 153 us
  blocking collectives  64.4 us (42%)
  Pallas kernels  36.3 us (24%)
  waiting for transfers between devices  29.2 us (19%)
  between operations  13.4 us (9%)
  matrix products  7 us (5%)
    all_gather x1, waiting for transfers between devices, body(): lax.all_gather(head_out, 'tp', axis=1, tiled=True)  29.2 us
    pallas_call x1, Pallas kernels, local_call(): pl.pallas_call(make_local_kernel(first_head_of), out_shape=(jax.ShapeDtyp...  28.4 us
    all_gather x1, blocking collectives, body(): mod_rows = lax.all_gather(summed[:4], 'tp', axis=1, tiled=True)  16.3 us
    all_to_all x1, blocking collectives, body(): lax.all_to_all(copies, SP, split_axis=0, concat_axis=0, tiled=True)  15.8 us
    all_to_all x1, blocking collectives, body(): lax.all_to_all(jnp.stack([ctx_map, lat_map], axis=1), 'sp_1', split_axis=...  12.4 us
    all_gather x1, blocking collectives, body(): all_totals = lax.all_gather(totals, 'sp_0', axis=0)  11.1 us
    all_to_all x1, blocking collectives, body(): lax.all_to_all(starts, 'sp_1', split_axis=0, concat_axis=0, tiled=True)  8.82 us
    dot_general x1, matrix products, body(): jnp.dot(lax.all_gather(head_out, 'tp', axis=1, tiled=True), out_weight, p...  3.72 us
  transfers between devices with their start and end apart: 1, of which 1 were waited for; matrix products, arithmetic and copies ran while one was open for 0% of the time, Pallas kernels for 0%

commit v1 on v0

v1 whole, which is shorter than its diff:
```python
import jax
import jax.numpy as jnp
from jax import lax
from jax.experimental import pallas as pl
from jax.experimental.pallas import tpu as pltpu
from jax.sharding import Mesh
from jax.sharding import PartitionSpec as P

HEAD_DIM = 128
SP = ("sp_0", "sp_1")
EPS = 0.0001
F32 = jnp.float32
BF16 = jnp.bfloat16
TILE = 128
MESH = pl.DeviceIdType.MESH
LEVELS = (1, 2, 3, 4, 5, 6)


def mm(a, b):
    return jnp.dot(a.astype(BF16), b.astype(BF16), preferred_element_type=F32)


def mm_nt(a, b):
    return lax.dot_general(a, b, (((1,), (1,)), ((), ())), preferred_element_type=F32)


def mm_tn(a, b):
    return lax.dot_general(a, b, (((0,), (0,)), ((), ())), preferred_element_type=F32)


def iota2(shape, dim):
    return lax.broadcasted_iota(jnp.int32, shape, dim)


def softplus(u):
    return jnp.maximum(u, 0.0) + jnp.log1p(jnp.exp(-jnp.abs(u)))


def inv_norm(rows_bf16):
    r = rows_bf16.astype(F32)
    return lax.rsqrt(jnp.sum(r * r, axis=-1, keepdims=True) + EPS)


def gate_rows(first_head, pre_ref, wb_ref, db_ref, lr_ref, rows_ref, n_lat, n_ctx):
    width = n_lat + TILE
    lane = iota2((8, width), 1)
    is_ctx = lane >= n_lat
    pos = jnp.where(is_ctx, lane - n_lat, lane)
    size = jnp.where(is_ctx, n_ctx, n_lat)
    valid = pos < size
    row = iota2((8, width), 0)
    rates = jnp.zeros((8, width), F32)
    logd = jnp.zeros((8, width), F32)
    for c in range(4):
        d, h = c // 2, c % 2
        head = first_head + h
        at = d * 16 + head
        w = pre_ref[pl.ds(at, 1), :] + wb_ref[d, head]
        u = pre_ref[pl.ds(32 + at, 1), :] + db_ref[d, head]
        rate = 1.0 / (1.0 + jnp.exp(-w))
        step = -jnp.exp(jnp.full((1, width), lr_ref[d, head], F32)) * softplus(u)
        rates = jnp.where(row == c, rate, rates)
        logd = jnp.where(row == c, step, logd)
    rates = jnp.where(valid, rates, 0.0)
    logd = jnp.where(valid, logd, 0.0)
    fwd = logd
    bwd = logd
    s = 1
    while s < n_lat:
        fwd = fwd + jnp.where(pos >= s, pltpu.roll(fwd, s, 1), 0.0)
        bwd = bwd + jnp.where(pos + s < size, pltpu.roll(bwd, width - s, 1), 0.0)
        s *= 2
    g = jnp.where(row < 2, fwd, bwd)
    g = jnp.where(valid, g, 0.0)
    whole_lat = jnp.sum(jnp.where(is_ctx, 0.0, logd), axis=1, keepdims=True)
    whole_ctx = jnp.sum(jnp.where(is_ctx, logd, 0.0), axis=1, keepdims=True)
    late = jnp.exp(jnp.where(is_ctx, whole_ctx, whole_lat) - g)
    eg = jnp.exp(g)
    parts = []
    for a in (rates, g, late, eg):
        up = pltpu.roll(pltpu.roll(a, n_ctx, 1), 6, 0)
        a = jnp.where(lane >= n_lat + n_ctx, up, a)
        parts.append(a)
    rows_ref[...] = jnp.zeros_like(rows_ref)
    for n, a in enumerate(parts):
        rows_ref[8 * n : 8 * n + 8, :] = a
    return jnp.exp(whole_lat), jnp.exp(whole_ctx)


def split_rows(x):
    hi = x.astype(BF16)
    lo = (x - hi.astype(F32)).astype(BF16)
    return hi, lo


def mul_precise(m_bf16, x):
    hi, lo = split_rows(x)
    n = x.shape[1]
    y = jnp.dot(m_bf16, jnp.concatenate([hi, lo], axis=1), preferred_element_type=F32)
    return y[:, :n] + y[:, n:]


def then(next_map, total):
    y = mul_precise(next_map[:, :TILE], total)
    zero = jnp.zeros((TILE, TILE), F32)
    return y + jnp.concatenate([zero, next_map[:, TILE:].astype(F32)], axis=1)


RATE, G, LATE, EG, KINV = 0, 8, 16, 24, 32


def remote(src, dst, send_sem, recv_sem, axis, peer):
    return pltpu.make_async_remote_copy(
        src_ref=src, dst_ref=dst, send_sem=send_sem, recv_sem=recv_sem, device_id={axis: peer}, device_id_type=MESH
    )


def greet(barrier, peers):
    for axis, peer in peers:
        pl.semaphore_signal(barrier, inc=1, device_id={axis: peer}, device_id_type=MESH)


def ring_peers(axis, size):
    me = lax.axis_index(axis)
    return [(axis, lax.rem(me + k, size)) for k in range(1, size)]


def project_kernel(
    cond_ref, cctx_ref, shift_ref, scale_ref, gate_ref, gain_ref, ww_ref, wd_ref,
    lat_hbm, ctx_hbm, wq_hbm, wk_hbm, wv_hbm,
    q_ref, k_ref, v_ref, pre_ref, gate_row_ref,
    lat_ref, ctx_ref, w_ref, load_sem, inv_ref, ab_ref, mod_ref,
    part_ref, sum_ref, own_ref, xbuf, zbuf, tbuf, send_sem, recv_sem,
):
    barrier = pltpu.get_barrier_semaphore()
    xs, zs, ts = ring_peers("sp_1", 4), ring_peers("sp_0", 4), ring_peers("tp", 8)
    greet(barrier, xs + zs + ts)
    loads = [
        pltpu.make_async_copy(src, dst, load_sem.at[n])
        for n, (src, dst) in enumerate(
            (
                (lat_hbm, lat_ref), (ctx_hbm, ctx_ref), (wk_hbm, w_ref.at[0]), (wv_hbm, w_ref.at[1]), (wq_hbm, w_ref.at[2]),
            )
        )
    ]
    for load in loads:
        load.start()
    n_lat, n_ctx = lat_ref.shape[0], ctx_ref.shape[0]
    u = jnp.concatenate([cond_ref[...].astype(F32), cctx_ref[...].astype(F32)], axis=0)
    silu = (u / (1.0 + jnp.exp(-u))).astype(BF16)
    part_ref[...] = jnp.zeros_like(part_ref)
    part_ref[0:2, :] = jnp.dot(silu, shift_ref[...], preferred_element_type=F32)
    part_ref[2:4, :] = jnp.dot(silu, scale_ref[...], preferred_element_type=F32)
    part_ref[4:5, :] = jnp.dot(silu, gate_ref[...], preferred_element_type=F32)[0:1]
    pl.semaphore_wait(barrier, len(xs + zs + ts))
    phase_x = [
        remote(part_ref, xbuf.at[n], send_sem.at[n], recv_sem.at[n], *peer) for n, peer in enumerate(xs)
    ]
    for copy in phase_x:
        copy.start()
    loads[0].wait()
    loads[1].wait()

    def norms(src_ref, base):
        def step(i, carry):
            x = src_ref[pl.ds(i * 16, 16), :].astype(F32)
            inv = lax.rsqrt(jnp.mean(x * x, axis=-1, keepdims=True) + EPS)
            inv_ref[pl.ds(base + i * 16, 16), :] = jnp.broadcast_to(inv, (16, TILE))
            return carry

        return step

    lax.fori_loop(0, n_lat // 16, norms(lat_ref, 0), 0)
    lax.fori_loop(0, n_ctx // 16, norms(ctx_ref, n_lat), 0)
    for copy in phase_x:
        copy.wait()
    sum_ref[...] = part_ref[...] + xbuf[0] + xbuf[1] + xbuf[2]
    phase_z = [
        remote(sum_ref, zbuf.at[n], send_sem.at[3 + n], recv_sem.at[3 + n], *peer) for n, peer in enumerate(zs)
    ]
    for copy in phase_z:
        copy.start()
    for copy in phase_z:
        copy.wait()
    whole = sum_ref[...] + zbuf[0] + zbuf[1] + zbuf[2]
    own_ref[...] = whole[0:4]
    gate_row_ref[...] = whole[4:5]
    t = lax.axis_index("tp")
    phase_t = [
        remote(own_ref, tbuf.at[t], send_sem.at[6 + n], recv_sem.at[6 + n], *peer) for n, peer in enumerate(ts)
    ]
    for copy in phase_t:
        copy.start()
    tbuf[t] = own_ref[...]
    pre_ref[...] = jnp.zeros_like(pre_ref)
    for copy in phase_t:
        copy.wait()
    own_cols = own_ref.shape[1]
    for n in range(8):
        cols = slice(n * own_cols, (n + 1) * own_cols)
        for s in range(2):
            ab_ref[2 * s, :, cols] = gain_ref[:, cols] * (1.0 + tbuf[n, 2 + s : 3 + s, :])
            ab_ref[2 * s + 1, :, cols] = tbuf[n, s : s + 1, :]

    def scaled(src_ref, base, s):
        def step(i, carry):
            x = src_ref[pl.ds(i * 16, 16), :].astype(F32)
            inv = inv_ref[pl.ds(base + i * 16, 16), 0:1]
            y = x * inv * ab_ref[2 * s] + ab_ref[2 * s + 1]
            mod_ref[pl.ds(base + i * 16, 16), :] = y.astype(BF16)
            return carry

        return step

    lax.fori_loop(0, n_lat // 16, scaled(lat_ref, 0, 0), 0)
    lax.fori_loop(0, n_ctx // 16, scaled(ctx_ref, n_lat, 1), 0)
    for n, w in enumerate((ww_ref, wd_ref)):
        r = slice(32 * n, 32 * n + 32)
        pre_ref[r, 0:n_lat] = mm_nt(w[...], mod_ref[0:n_lat, :]).astype(BF16).astype(F32)
        pre_ref[r, n_lat : n_lat + n_ctx] = mm_nt(w[...], mod_ref[n_lat:, :]).astype(BF16).astype(F32)
    for load in loads[2:]:
        load.wait()
    k_ref[...] = mm(mod_ref[...], w_ref[0]).astype(BF16)
    v_ref[...] = mm(mod_ref[...], w_ref[1]).astype(BF16)
    q_ref[...] = mm(mod_ref[0:n_lat, :], w_ref[2]).astype(BF16)


def inverses(ad_ref, t_ref, base, count):
    xor = iota2((TILE, TILE), 0) ^ iota2((TILE, TILE), 1)
    eye = jnp.where(xor == 0, 1.0, 0.0)
    ts = []
    for n in range(count):
        a = ad_ref[base + n].astype(F32)
        ts.append((eye - jnp.where(xor == 1, a, 0.0)).astype(BF16))
    for level in LEVELS:
        xs = []
        for n in range(count):
            off = jnp.where((xor >> level) == 1, ad_ref[base + n].astype(F32), 0.0).astype(BF16)
            xs.append(mm(ts[n], off).astype(BF16))
        ts = [(t.astype(F32) - mm(x, t)).astype(BF16) for x, t in zip(xs, ts)]
    for n in range(count):
        t_ref[base + n] = ts[n]


def token_kernel(
    q_ref, k_ref, v_ref, pre_ref, gate_row_ref, gain_ref, wb_ref, db_ref, lr_ref, lat_hbm, ow_hbm,
    out_ref,
    ow_ref, res_ref, load_sem,
    rows_ref, cols_ref, gk_ref, qk_ref, ad_ref, t_ref, ao_ref, p_ref, x_ref, xl_ref, o1_ref, q2_ref,
    lat_map, ctx_map, lat_all, ctx_all, prefix_ref, lat_total, ctx_total, lat_totals, ctx_totals,
    start_ref, mine_ref, ho_ref, send_sem, recv_sem, ho_send, ho_recv,
):
    n_lat = q_ref.shape[0]
    n_ctx = k_ref.shape[0] - n_lat
    blocks = n_lat // TILE
    width = n_lat + TILE
    x_at, z_at, t_at = lax.axis_index("sp_1"), lax.axis_index("sp_0"), lax.axis_index("tp")
    y_at, core = t_at // 2, lax.rem(t_at, 2)
    up = lax.rem(y_at + 1, 4) * 2 + core
    down = lax.rem(y_at + 3, 4) * 2 + core
    across = lax.rem(y_at + 2, 4) * 2 + core
    mate = y_at * 2 + 1 - core
    barrier = pltpu.get_barrier_semaphore()
    xs, zs = ring_peers("sp_1", 4), ring_peers("sp_0", 4)
    greet(barrier, xs + zs + [("tp", up), ("tp", down), ("tp", mate)])
    own_cols = out_ref.shape[1]
    load_w = pltpu.make_async_copy(ow_hbm, ow_ref, load_sem.at[0])
    load_r = pltpu.make_async_copy(
        lat_hbm.at[:, pl.ds(pl.multiple_of(t_at * own_cols, own_cols), own_cols)], res_ref, load_sem.at[1]
    )
    load_w.start()
    load_r.start()

    dec_lat, dec_ctx = gate_rows(t_at * 2, pre_ref, wb_ref, db_ref, lr_ref, rows_ref, n_lat, n_ctx)
    for b in range(blocks + 1):
        cols_ref[b * TILE : (b + 1) * TILE, :] = jnp.transpose(rows_ref[:, b * TILE : (b + 1) * TILE])

    def kcols(h):
        return k_ref[0:n_lat, h * TILE : (h + 1) * TILE]

    def kctx(h):
        kc = k_ref[n_lat : n_lat + n_ctx, h * TILE : (h + 1) * TILE]
        return jnp.concatenate([kc, kc], axis=0)

    def vctx(h):
        vc = v_ref[n_lat : n_lat + n_ctx, h * TILE : (h + 1) * TILE]
        return jnp.concatenate([vc, vc], axis=0)

    kinv = []
    for h in range(2):
        kinv.append(jnp.concatenate([inv_norm(kcols(h)), inv_norm(kctx(h))], axis=0))
    lane128 = iota2((width, TILE), 1)
    both = jnp.where(lane128 == 0, kinv[0], jnp.where(lane128 == 1, kinv[1], 0.0))
    ii = iota2((TILE, TILE), 0)
    jj = iota2((TILE, TILE), 1)
    xor = ii ^ jj
    for b in range(blocks + 1):
        rows_ref[:, b * TILE : (b + 1) * TILE] = jnp.where(
            ii < KINV,
            rows_ref[:, b * TILE : (b + 1) * TILE],
            pltpu.roll(jnp.transpose(both[b * TILE : (b + 1) * TILE, :]), KINV, 0),
        )

    for h in range(2):
        kc = kctx(h)
        g2 = mm_nt(kc, kc) * kinv[h][n_lat:] * rows_ref[KINV + h : KINV + h + 1, n_lat:]
        keep = jnp.where(ii < n_ctx, jnp.where(jj < ii, 1, 0), jnp.where(jj > ii, 1, 0))
        keep = jnp.where((ii < n_ctx) == (jj < n_ctx), keep, 0) == 1
        sp = cols_ref[n_lat:, G + h : G + h + 1] - rows_ref[G + h : G + h + 1, n_lat:]
        dm = jnp.where(keep, jnp.exp(jnp.where(keep, sp, 0.0)), 0.0)
        ad_ref[4 * blocks + h] = (g2 * dm * cols_ref[n_lat:, RATE + h : RATE + h + 1]).astype(BF16)
    inverses(ad_ref, t_ref, 4 * blocks, 2)
    for h in range(2):
        ci = kinv[h][n_lat:]
        cr = slice(n_lat, n_lat + TILE)
        rate = cols_ref[cr, RATE + h : RATE + h + 1]
        eg = cols_ref[cr, EG + h : EG + h + 1]
        late = cols_ref[cr, LATE + h : LATE + h + 1]
        kc = kctx(h)
        b = jnp.concatenate([vctx(h).astype(F32) * rate, kc.astype(F32) * (rate * eg * ci)], axis=1)
        x = mm(t_ref[4 * blocks + h], b)
        xl = (x * (late * ci)).astype(BF16)
        for d in range(2):
            c = d * 2 + h
            m = mm_tn(kc[0:n_ctx], xl[d * n_ctx : (d + 1) * n_ctx])
            diag = jnp.where(xor == 0, dec_ctx[c : c + 1, :], 0.0)
            ctx_map[c] = jnp.concatenate([diag - m[:, TILE:], m[:, :TILE]], axis=1).astype(BF16)

    pl.semaphore_wait(barrier, 9)

    def to_row(base, maps, everyone):
        copies = [
            remote(maps.at[peer], everyone.at[x_at], send_sem.at[base + n], recv_sem.at[base + n], axis, peer)
            for n, (axis, peer) in enumerate(xs)
        ]
        for copy in copies:
            copy.start()
        everyone[x_at] = maps[x_at]
        return copies

    def to_column(base, total, everyone):
        copies = [
            remote(total, everyone.at[z_at], send_sem.at[base + n], recv_sem.at[base + n], axis, peer)
            for n, (axis, peer) in enumerate(zs)
        ]
        for copy in copies:
            copy.start()
        everyone[z_at] = total[...]
        return copies

    ctx_rows = to_row(0, ctx_map, ctx_all)

    qinvs = []
    for h in range(2):
        qh = q_ref[0:n_lat, h * TILE : (h + 1) * TILE]
        qinv = inv_norm(qh) * (HEAD_DIM**-0.5)
        qinvs.append(qinv)
        krow = rows_ref[KINV + h : KINV + h + 1, 0:n_lat]
        gk_ref[h] = mm_nt(kcols(h), kcols(h)) * kinv[h][0:n_lat] * krow
        qk_ref[h] = mm_nt(qh, kcols(h)) * qinv * krow
    for c in range(4):
        d, h = c // 2, c % 2
        for i in range(blocks):
            ri = cols_ref[i * TILE : (i + 1) * TILE, RATE + c : RATE + c + 1]
            gi = cols_ref[i * TILE : (i + 1) * TILE, G + c : G + c + 1]
            for j in range(blocks):
                if (d == 0 and j > i) or (d == 1 and j < i):
                    continue
                at = (slice(i * TILE, (i + 1) * TILE), slice(j * TILE, (j + 1) * TILE))
                sp = gi - rows_ref[G + c : G + c + 1, j * TILE : (j + 1) * TILE]
                if i == j:
                    keep = (ii >= jj) if d == 0 else (ii <= jj)
                    dm = jnp.where(keep, jnp.exp(jnp.where(keep, sp, 0.0)), 0.0)
                else:
                    dm = jnp.exp(sp)
                a = gk_ref[(h, *at)] * dm * ri
                if i == j:
                    ad_ref[c * blocks + i] = jnp.where(ii == jj, 0.0, a).astype(BF16)
                else:
                    ao_ref[(c, *at)] = a.astype(BF16)
                p_ref[(c, *at)] = (qk_ref[(h, *at)] * dm).astype(BF16)

    def invert(part, carry):
        inverses(ad_ref, t_ref, part * 8, 8)
        return carry

    lax.fori_loop(0, 4 * blocks // 8, invert, 0)

    backwards = x_at >= 2

    def place(n, size):
        return jnp.where(backwards, size - 1 - n, n)

    for copy in ctx_rows:
        copy.wait()
    total = ctx_all[place(0, 4)].astype(F32)
    for n in range(1, 4):
        total = then(ctx_all[place(n, 4)], total)
    ctx_total[...] = total.astype(BF16)
    ctx_columns = to_column(3, ctx_total, ctx_totals)

    for c in range(4):
        d, h = c // 2, c % 2
        order = list(range(blocks)) if d == 0 else list(reversed(range(blocks)))
        for n, i in enumerate(order):
            r = slice(i * TILE, (i + 1) * TILE)
            rate = cols_ref[r, RATE + c : RATE + c + 1]
            eg = cols_ref[r, EG + c : EG + c + 1]
            late = cols_ref[r, LATE + c : LATE + c + 1]
            ki = kinv[h][r]
            vi = v_ref[r, h * TILE : (h + 1) * TILE].astype(F32) * rate
            wi = k_ref[r, h * TILE : (h + 1) * TILE].astype(F32) * (rate * eg * ki)
            b = jnp.concatenate([vi, wi], axis=1)
            if n > 0:
                done = slice(0, i * TILE) if d == 0 else slice((i + 1) * TILE, n_lat)
                b = b - mm(ao_ref[c, r, done], x_ref[c, done, :])
            x = mm(t_ref[c * blocks + i], b)
            x_ref[c, r, :] = x.astype(BF16)
            xl_ref[c, r, :] = (x * (late * ki)).astype(BF16)
    for c in range(4):
        m = mm_tn(kcols(c % 2), xl_ref[c])
        diag = jnp.where(xor == 0, dec_lat[c : c + 1, :], 0.0)
        lat_map[c] = jnp.concatenate([diag - m[:, TILE:], m[:, :TILE]], axis=1).astype(BF16)
    lat_rows = to_row(6, lat_map, lat_all)

    for h in range(2):
        o1 = []
        for d in range(2):
            c = d * 2 + h
            for i in range(blocks):
                r = slice(i * TILE, (i + 1) * TILE)
                seen = slice(0, (i + 1) * TILE) if d == 0 else slice(i * TILE, n_lat)
                ow = mm(p_ref[c, r, seen], x_ref[c, seen, :])
                qi = q_ref[r, h * TILE : (h + 1) * TILE].astype(F32)
                early = qi * (cols_ref[r, EG + c : EG + c + 1] * qinvs[h][r])
                q2_ref[h, r, d * TILE : (d + 1) * TILE] = (early - ow[:, TILE:]).astype(BF16)
                if d == 0:
                    o1.append(ow[:, :TILE])
                else:
                    o1_ref[h, r, :] = o1[i] + ow[:, :TILE]

    for copy in ctx_columns:
        copy.wait()
    state = None
    for n in range(4):
        one = ctx_totals[place(n, 4)]
        off = one[:, TILE:].astype(F32)
        state = off if n == 0 else mul_precise(one[:, :TILE], state) + off
    for copy in lat_rows:
        copy.wait()
    total = None
    for n in range(4):
        at = place(n, 4)
        one = lat_all[at]
        if n > 0:
            prefix_ref[at] = total
        total = one.astype(F32) if n == 0 else then(one, total)
    lat_total[...] = total.astype(BF16)
    lat_columns = to_column(9, lat_total, lat_totals)
    for copy in lat_columns:
        copy.wait()
    z_place = place(z_at, 4)
    for n in range(3):
        one = lat_totals[place(n, 4)]
        new = mul_precise(one[:, :TILE], state) + one[:, TILE:].astype(F32)
        state = jnp.where(n < z_place, new, state)
    start_ref[place(0, 4)] = state.astype(BF16)
    for n in range(1, 4):
        at = place(n, 4)
        mk = prefix_ref[at]
        hi, lo = split_rows(mk[:, :TILE])
        start_ref[at] = (mul_precise(hi, state) + mm(lo, state) + mk[:, TILE:]).astype(BF16)
    starts = to_row(12, start_ref, mine_ref)
    for copy in starts:
        copy.wait()

    half = n_lat // 2
    A, B = slice(0, half), slice(half, n_lat)

    def finish(r):
        for h in range(2):
            both_s = jnp.concatenate([mine_ref[h], mine_ref[2 + h]], axis=0)
            y = o1_ref[h, r, :] + jnp.dot(q2_ref[h, r, :], both_s, preferred_element_type=F32)
            y = y * lax.rsqrt(jnp.mean(y * y, axis=-1, keepdims=True) + EPS) * gain_ref[...]
            ho_ref[t_at, r, h * TILE : (h + 1) * TILE] = y.astype(BF16)

    def hand(n, block, r, peer):
        copy = remote(ho_ref.at[block, r], ho_ref.at[block, r], ho_send.at[n], ho_recv.at[n], "tp", peer)
        copy.start()
        return copy

    hands = {}
    finish(A)
    hands[0] = hand(0, t_at, A, up)
    hands[4] = hand(4, t_at, A, mate)
    finish(B)
    hands[3] = hand(3, t_at, B, down)
    hands[1] = hand(1, t_at, B, up)
    hands[2] = hand(2, t_at, A, down)
    hands[5] = hand(5, t_at, B, mate)
    load_w.wait()
    load_r.wait()
    depth = 2 * TILE

    def add(block):
        w = ow_ref[pl.ds(pl.multiple_of(block * depth, depth), depth), :]
        return jnp.dot(ho_ref[block], w, preferred_element_type=F32)

    hands[0].wait_recv()
    hands[6] = hand(6, down, A, up)
    hands[8] = hand(8, down, A, mate)
    hands[3].wait_recv()
    hands[7] = hand(7, up, B, down)
    hands[11] = hand(11, up, B, mate)
    hands[4].wait_recv()
    hands[5].wait_recv()
    acc = add(t_at) + add(mate)
    hands[1].wait_recv()
    hands[9] = hand(9, down, B, mate)
    hands[2].wait_recv()
    hands[10] = hand(10, up, A, mate)
    acc = acc + add(down) + add(up)
    hands[6].wait_recv()
    hands[12] = hand(12, across, A, mate)
    hands[7].wait_recv()
    hands[13] = hand(13, across, B, mate)
    for n in range(8, 12):
        hands[n].wait_recv()

    def other(block):
        return block + 1 - 2 * core

    acc = acc + add(other(down)) + add(other(up)) + add(across)
    hands[12].wait_recv()
    hands[13].wait_recv()
    acc = acc + add(other(across))
    out_ref[...] = (res_ref[...].astype(F32) + gate_row_ref[...] * acc).astype(BF16)
    for n in range(14):
        hands[n].wait_send()


def body(
    latent, context, condition, context_condition, shift_weight, scale_weight, gate_weight, norm_gain,
    query_weight, key_weight, value_weight, write_weight, decay_weight, write_bias, decay_bias, log_rate,
    head_gain, out_weight,
):
    n_lat, d = latent.shape
    n_ctx = context.shape[0]
    n_all = n_lat + n_ctx
    own_cols = gate_weight.shape[1]
    pair = query_weight.shape[1]
    blocks = n_lat // TILE
    tiles = 4 * blocks + 2
    width = n_lat + TILE
    vm = pl.BlockSpec(memory_space=pltpu.VMEM)
    sm = pl.BlockSpec(memory_space=pltpu.SMEM)
    hb = pl.BlockSpec(memory_space=pl.ANY)
    gates = [jnp.transpose(w, (1, 2, 0)).reshape(32, -1) for w in (write_weight, decay_weight)]
    shape = jax.ShapeDtypeStruct
    q, k, v, pre, gate_row = pl.pallas_call(
        project_kernel,
        out_shape=(
            shape((n_lat, pair), BF16), shape((n_all, pair), BF16), shape((n_all, pair), BF16),
            shape((64, width), F32), shape((1, own_cols), F32),
        ),
        in_specs=[vm] * 8 + [hb] * 5,
        out_specs=(vm,) * 5,
        scratch_shapes=[
            pltpu.VMEM((n_lat, d), BF16), pltpu.VMEM((n_ctx, d), BF16), pltpu.VMEM((3, d, pair), BF16),
            pltpu.SemaphoreType.DMA((5,)), pltpu.VMEM((n_all, TILE), F32), pltpu.VMEM((4, 1, d), F32),
            pltpu.VMEM((n_all, d), BF16), pltpu.VMEM((8, own_cols), F32), pltpu.VMEM((8, own_cols), F32),
            pltpu.VMEM((4, own_cols), F32), pltpu.VMEM((3, 8, own_cols), F32), pltpu.VMEM((3, 8, own_cols), F32),
            pltpu.VMEM((8, 4, own_cols), F32), pltpu.SemaphoreType.DMA((13,)), pltpu.SemaphoreType.DMA((13,)),
        ],
        compiler_params=pltpu.CompilerParams(
            collective_id=0, has_side_effects=True, vmem_limit_bytes=48 * 1024 * 1024
        ),
        name="project",
    )(
        condition.reshape(1, -1), context_condition.reshape(1, -1), shift_weight, scale_weight, gate_weight,
        norm_gain.reshape(1, -1), *gates, latent, context, query_weight, key_weight, value_weight,
    )
    one_map = (TILE, 2 * TILE)
    return pl.pallas_call(
        token_kernel,
        out_shape=shape((n_lat, own_cols), BF16),
        in_specs=[vm] * 6 + [sm] * 3 + [hb] * 2,
        out_specs=vm,
        scratch_shapes=[
            pltpu.VMEM(out_weight.shape, BF16), pltpu.VMEM((n_lat, own_cols), BF16), pltpu.SemaphoreType.DMA((2,)),
            pltpu.VMEM((TILE, width), F32), pltpu.VMEM((width, TILE), F32),
            pltpu.VMEM((2, n_lat, n_lat), F32), pltpu.VMEM((2, n_lat, n_lat), F32),
            pltpu.VMEM((tiles, TILE, TILE), BF16), pltpu.VMEM((tiles, TILE, TILE), BF16),
            pltpu.VMEM((4, n_lat, n_lat), BF16), pltpu.VMEM((4, n_lat, n_lat), BF16),
            pltpu.VMEM((4, n_lat, 2 * TILE), BF16), pltpu.VMEM((4, n_lat, 2 * TILE), BF16),
            pltpu.VMEM((2, n_lat, TILE), F32), pltpu.VMEM((2, n_lat, 2 * TILE), BF16),
            pltpu.VMEM((4, *one_map), BF16), pltpu.VMEM((4, *one_map), BF16),
            pltpu.VMEM((4, *one_map), BF16), pltpu.VMEM((4, *one_map), BF16),
            pltpu.VMEM((4, *one_map), F32), pltpu.VMEM(one_map, BF16), pltpu.VMEM(one_map, BF16),
            pltpu.VMEM((4, *one_map), BF16), pltpu.VMEM((4, *one_map), BF16),
            pltpu.VMEM((4, TILE, TILE), BF16), pltpu.VMEM((4, TILE, TILE), BF16),
            pltpu.VMEM((8, n_lat, pair), BF16),
            pltpu.SemaphoreType.DMA((15,)), pltpu.SemaphoreType.DMA((15,)),
            pltpu.SemaphoreType.DMA((14,)), pltpu.SemaphoreType.DMA((14,)),
        ],
        compiler_params=pltpu.CompilerParams(
            collective_id=1, has_side_effects=True, vmem_limit_bytes=48 * 1024 * 1024
        ),
        name="tokens",
    )(q, k, v, pre, gate_row, head_gain.reshape(1, -1), write_bias, decay_bias, log_rate, latent, out_weight)


def solution(mesh):
    torus = Mesh(mesh.devices.reshape(4, 4, mesh.shape["tp"]), ("sp_0", "sp_1", "tp"))
    placed = (
        P(SP, None), P(SP, None), P(SP), P(SP), P(SP, "tp"), P(SP, "tp"), P(SP, "tp"), P(),
        P(None, "tp"), P(None, "tp"), P(None, "tp"), P(), P(), P(), P(), P(), P(), P(None, "tp"),
    )
    return jax.shard_map(body, mesh=torus, in_specs=placed, out_specs=P(SP, "tp"), check_vma=False)
```

time: 154 us -> 82.4 us (0.54)
  blocking collectives: 64.4 us -> 0 us
  Pallas kernels: 36.3 us -> 71.7 us
  waiting for transfers between devices: 29.2 us -> 0 us
  between operations: 13.4 us -> 0.08 us
  local copies, waits for them, and re-layouts: 1.5 us -> 10.2 us
  matrix products: 7 us -> 0 us
    all_to_all x3 -> x0, blocking collectives: 36.9 us -> none  [the longest x1 15.8 us: body(): lax.all_to_all(copies, SP, split_axis=0, concat_axis=0, tiled=True)]
    pallas_call x4 -> x2, Pallas kernels: 36.3 us -> 71.7 us  [the longest x1 41.1 us: body(): pl.pallas_call(token_kernel, out_shape=shape((n_lat, own_cols), BF16), in...]
    all_gather x1 -> x0, waiting for transfers between devices: 29.2 us -> none  [body(): lax.all_gather(head_out, 'tp', axis=1, tiled=True)]
    all_gather x2 -> x0, blocking collectives: 27.4 us -> none  [the longest x1 16.3 us: body(): mod_rows = lax.all_gather(summed[:4], 'tp', axis=1, tiled=True)]
    unnamed x2 -> x27, local copies, waits for them, and re-layouts: 0.01 us -> 8.91 us
    dot_general x4 -> x0, matrix products: 7 us -> none  [the longest x1 3.72 us: body(): jnp.dot(lax.all_gather(head_out, 'tp', axis=1, tiled=True), out_weight, p...]
  transfers between devices with their start and end apart: 1 -> 0, of which waited for: 1 -> 0; matrix products, arithmetic and copies ran while one was open for 0% -> 0% of each run, Pallas kernels for 0% -> 0%
where the time goes in v1:
time: 82.4 us; the launch traced here: 82 us
  Pallas kernels  71.7 us (87%)
  local copies, waits for them, and re-layouts  10.2 us (12%)
    pallas_call x1, Pallas kernels, body(): pl.pallas_call(token_kernel, out_shape=shape((n_lat, own_cols), BF16), in...  41.1 us
    pallas_call x1, Pallas kernels, body(): pl.pallas_call(project_kernel, out_shape=(shape((n_lat, pair), BF16), sha...  30.6 us
    unnamed x27, local copies, waits for them, and re-layouts  8.91 us

profile of v1, /device:TPU:1, one launch (start us, length us, event | category | flops | bytes accessed | tf_op | source)
XLA Modules:
  0.0 82.0 jit_solution(14423941243416050803)
XLA Ops:
  0.0 0.7 reshape.18.cond_ref
  0.7 0.7 reshape.19.cctx_ref
  1.3 0.0 copy-start
  1.3 1.6 %copy-done = bf16[4096,256]{1,0:T(8,128)(2,1)S(1)} copy-done((bf16[4096,256]{1,0:T(8,128)(2,1)S(1)}, bf16[4096,256]{1,0:T(8,128)(2,1)}, u32[]{:S(2)}) %copy-start) | copy-done | bytes 2097176
  2.9 0.0 copy-start.2
  2.9 1.0 %copy-done.2 = bf16[64,4096]{1,0:T(8,128)(2,1)S(1)} copy-done((bf16[64,4096]{1,0:T(8,128)(2,1)S(1)}, bf16[64,4096]{1,0:T(8,128)(2,1)}, u32[]{:S(2)}) %copy-start.2) | copy-done | bytes 524312
  4.0 0.0 copy-start.3
  4.0 0.9 %copy-done.3 = bf16[256,512]{1,0:T(8,128)(2,1)S(1)} copy-done((bf16[256,512]{1,0:T(8,128)(2,1)S(1)}, bf16[256,512]{1,0:T(8,128)(2,1)}, u32[]{:S(2)}) %copy-start.3) | copy-done | bytes 262168
  4.9 0.0 copy-start.4
  4.9 0.9 %copy-done.4 = bf16[256,512]{1,0:T(8,128)(2,1)S(1)} copy-done((bf16[256,512]{1,0:T(8,128)(2,1)S(1)}, bf16[256,512]{1,0:T(8,128)(2,1)}, u32[]{:S(2)}) %copy-start.4) | copy-done | bytes 262168
  5.9 0.0 copy-start.5
  5.9 0.9 %copy-done.5 = bf16[256,512]{1,0:T(8,128)(2,1)S(1)} copy-done((bf16[256,512]{1,0:T(8,128)(2,1)S(1)}, bf16[256,512]{1,0:T(8,128)(2,1)}, u32[]{:S(2)}) %copy-start.5) | copy-done | bytes 262168
  6.8 0.9 %copy-done.6 = bf16[4096,2,16]{0,2,1:T(8,128)(2,1)S(1)} copy-done((bf16[4096,2,16]{0,2,1:T(8,128)(2,1)S(1)}, bf16[4096,2,16]{0,2,1:T(8,128)(2,1)}, u32[]{:S(2)}) %copy-start.6) | copy-done | bytes 262168
  7.8 0.9 %copy-done.7 = bf16[4096,2,16]{0,2,1:T(8,128)(2,1)S(1)} copy-done((bf16[4096,2,16]{0,2,1:T(8,128)(2,1)S(1)}, bf16[4096,2,16]{0,2,1:T(8,128)(2,1)}, u32[]{:S(2)}) %copy-start.7) | copy-done | bytes 262168
  8.7 0.7 copy-done.8
  9.4 0.0 copy-start.12
  9.4 30.6 %project.1 = (bf16[512,256]{1,0:T(8,128)(2,1)S(1)}, bf16[576,256]{1,0:T(8,128)(2,1)S(1)}, bf16[576,256]{1,0:T(8,128)(2,1)S(1)}, f32[64,640]{1,0:T(8,128)S(1)}, f32[1,512]{1,0:T(1,128)S(1)}) custom-call(bf16[1,256]{1,0:T(2,128)(2,1)S(1)} %reshape.18.cond_ref, bf16[1,256]{1,0:T(2,128)(2,1)S(1)} %reshape.19.cctx_ref, bf16[256,512]{1,0:T(8,128)(2,1)S(1)} %copy-done.3, ...), custom_call_target="tpu_custom_call" | custom-call | tf_op jit(solution)/shard_map/project/pallas_call | solution.py:560
  40.0 0.0 copy-done.1
  40.0 0.0 copy-done.9
  40.0 0.0 copy-done.10
  40.0 0.0 copy-done.11
  40.0 0.0 copy-done.12
  40.1 41.1 %tokens.1 = bf16[512,512]{1,0:T(8,128)(2,1)S(1)} custom-call(bf16[512,256]{1,0:T(8,128)(2,1)S(1)} %get-tuple-element.10.q_ref, bf16[576,256]{1,0:T(8,128)(2,1)S(1)} %get-tuple-element.11.k_ref, bf16[576,256]{1,0:T(8,128)(2,1)S(1)} %get-tuple-element.12.v_ref, f32[64,640]{1,0:T(8,128)S(1)} %get-tuple-element.13.pre_ref, ...), custom_call_target="tpu_custom_call" | custom-call | tf_op jit(solution)/shard_map/tokens/pallas_call | solution.py:584
  81.2 0.8 copy.20
  (7 shorter events, 0.0 us)
Async XLA Ops:
  1.3 1.6 %copy-start = (bf16[4096,256]{1,0:T(8,128)(2,1)S(1)}, bf16[4096,256]{1,0:T(8,128)(2,1)}, u32[]{:S(2)}) copy-start(bf16[4096,256]{1,0:T(8,128)(2,1)} %wq_hbm.1) | copy-start | bytes 6291460
  2.9 1.0 %copy-start.2 = (bf16[64,4096]{1,0:T(8,128)(2,1)S(1)}, bf16[64,4096]{1,0:T(8,128)(2,1)}, u32[]{:S(2)}) copy-start(bf16[64,4096]{1,0:T(8,128)(2,1)} %ctx_hbm.1) | copy-start | bytes 1572868
  4.0 0.9 %copy-start.3 = (bf16[256,512]{1,0:T(8,128)(2,1)S(1)}, bf16[256,512]{1,0:T(8,128)(2,1)}, u32[]{:S(2)}) copy-start(bf16[256,512]{1,0:T(8,128)(2,1)} %shift_ref.1) | copy-start | bytes 786436
  4.9 0.9 %copy-start.4 = (bf16[256,512]{1,0:T(8,128)(2,1)S(1)}, bf16[256,512]{1,0:T(8,128)(2,1)}, u32[]{:S(2)}) copy-start(bf16[256,512]{1,0:T(8,128)(2,1)} %scale_ref.1) | copy-start | bytes 786436
  5.9 0.9 %copy-start.5 = (bf16[256,512]{1,0:T(8,128)(2,1)S(1)}, bf16[256,512]{1,0:T(8,128)(2,1)}, u32[]{:S(2)}) copy-start(bf16[256,512]{1,0:T(8,128)(2,1)} %gate_ref.1) | copy-start | bytes 786436
  6.8 0.9 %copy-start.6 = (bf16[4096,2,16]{0,2,1:T(8,128)(2,1)S(1)}, bf16[4096,2,16]{0,2,1:T(8,128)(2,1)}, u32[]{:S(2)}) copy-start(bf16[4096,2,16]{0,2,1:T(8,128)(2,1)} %param.29) | copy-start | bytes 786436
  7.8 0.9 %copy-start.7 = (bf16[4096,2,16]{0,2,1:T(8,128)(2,1)S(1)}, bf16[4096,2,16]{0,2,1:T(8,128)(2,1)}, u32[]{:S(2)}) copy-start(bf16[4096,2,16]{0,2,1:T(8,128)(2,1)} %param.30) | copy-start | bytes 786436
  8.7 0.7 copy-start.8
  9.4 30.6 %copy-start.1 = (bf16[2048,512]{1,0:T(8,128)(2,1)S(1)}, bf16[2048,512]{1,0:T(8,128)(2,1)}, u32[]{:S(2)}) copy-start(bf16[2048,512]{1,0:T(8,128)(2,1)} %ow_hbm.1) | copy-start | bytes 6291460
  9.4 30.6 %copy-start.9 = (f32[2,16]{1,0:T(2,128)S(1)}, f32[2,16]{1,0:T(2,128)}, u32[]{:S(2)}) copy-start(f32[2,16]{1,0:T(2,128)} %wb_ref.1) | copy-start | bytes 388
  9.4 30.6 %copy-start.10 = (f32[2,16]{1,0:T(2,128)S(1)}, f32[2,16]{1,0:T(2,128)}, u32[]{:S(2)}) copy-start(f32[2,16]{1,0:T(2,128)} %db_ref.1) | copy-start | bytes 388
  9.4 30.6 %copy-start.11 = (f32[2,16]{1,0:T(2,128)S(1)}, f32[2,16]{1,0:T(2,128)}, u32[]{:S(2)}) copy-start(f32[2,16]{1,0:T(2,128)} %lr_ref.1) | copy-start | bytes 388
  9.4 30.6 %copy-start.12 = (f32[128]{0:T(128)S(1)}, f32[128]{0:T(128)}, u32[]{:S(2)}) copy-start(f32[128]{0:T(128)} %param.34) | copy-start | bytes 1540

commit v2 on v1

--- a/solution.py
+++ b/solution.py
@@ -101,7 +101,7 @@
 
 
 def then(next_map, total):
-    y = mul_precise(next_map[:, :TILE], total)
+    y = mm(next_map[:, :TILE], total)
     zero = jnp.zeros((TILE, TILE), F32)
     return y + jnp.concatenate([zero, next_map[:, TILE:].astype(F32)], axis=1)
 
@@ -126,40 +126,62 @@
 
 
 def project_kernel(
-    cond_ref, cctx_ref, shift_ref, scale_ref, gate_ref, gain_ref, ww_ref, wd_ref,
+    cond_hbm, cctx_hbm, shift_hbm, scale_hbm, gate_hbm, gain_hbm, ww_hbm, wd_hbm,
     lat_hbm, ctx_hbm, wq_hbm, wk_hbm, wv_hbm,
     q_ref, k_ref, v_ref, pre_ref, gate_row_ref,
-    lat_ref, ctx_ref, w_ref, load_sem, inv_ref, ab_ref, mod_ref,
+    cond_ref, cctx_ref, mod_w_ref, gain_ref, wg_ref, lat_ref, ctx_ref, w_ref, load_sem,
+    inv_ref, piece_ref, acc_ref, pre_acc,
     part_ref, sum_ref, own_ref, xbuf, zbuf, tbuf, send_sem, recv_sem,
 ):
     barrier = pltpu.get_barrier_semaphore()
-    xs, zs, ts = ring_peers("sp_1", 4), ring_peers("sp_0", 4), ring_peers("tp", 8)
-    greet(barrier, xs + zs + ts)
+    t = lax.axis_index("tp")
+    y_at, core = t // 2, lax.rem(t, 2)
+    up = lax.rem(y_at + 1, 4) * 2 + core
+    down = lax.rem(y_at + 3, 4) * 2 + core
+    across = lax.rem(y_at + 2, 4) * 2 + core
+
+    def other(block):
+        return block + 1 - 2 * core
+
+    targets = [other(t), up, down, other(up), other(down), across, other(across)]
+    sources = [other(t), down, up, other(down), other(up), across, other(across)]
+    xs, zs = ring_peers("sp_1", 4), ring_peers("sp_0", 4)
+    greet(barrier, xs + zs + [("tp", peer) for peer in targets])
     loads = [
         pltpu.make_async_copy(src, dst, load_sem.at[n])
         for n, (src, dst) in enumerate(
             (
-                (lat_hbm, lat_ref), (ctx_hbm, ctx_ref), (wk_hbm, w_ref.at[0]), (wv_hbm, w_ref.at[1]), (wq_hbm, w_ref.at[2]),
+                (cond_hbm, cond_ref), (cctx_hbm, cctx_ref), (shift_hbm, mod_w_ref.at[0]), (scale_hbm, mod_w_ref.at[1]),
+                (gate_hbm, mod_w_ref.at[2]), (lat_hbm, lat_ref), (ctx_hbm, ctx_ref), (gain_hbm, gain_ref),
+                (ww_hbm, wg_ref.at[0:32]), (wd_hbm, wg_ref.at[32:64]),
+                (wk_hbm, w_ref.at[0]), (wv_hbm, w_ref.at[1]), (wq_hbm, w_ref.at[2]),
             )
         )
     ]
     for load in loads:
         load.start()
     n_lat, n_ctx = lat_ref.shape[0], ctx_ref.shape[0]
-    u = jnp.concatenate([cond_ref[...].astype(F32), cctx_ref[...].astype(F32)], axis=0)
+    n_all = n_lat + n_ctx
+    acc_ref[...] = jnp.zeros_like(acc_ref)
+    pre_acc[...] = jnp.zeros_like(pre_acc)
+    part_ref[...] = jnp.zeros_like(part_ref)
+    for load in loads[:5]:
+        load.wait()
+    u = jnp.concatenate(
+        [cond_ref[...].astype(F32).reshape(1, -1), cctx_ref[...].astype(F32).reshape(1, -1)], axis=0
+    )
     silu = (u / (1.0 + jnp.exp(-u))).astype(BF16)
-    part_ref[...] = jnp.zeros_like(part_ref)
-    part_ref[0:2, :] = jnp.dot(silu, shift_ref[...], preferred_element_type=F32)
-    part_ref[2:4, :] = jnp.dot(silu, scale_ref[...], preferred_element_type=F32)
-    part_ref[4:5, :] = jnp.dot(silu, gate_ref[...], preferred_element_type=F32)[0:1]
-    pl.semaphore_wait(barrier, len(xs + zs + ts))
+    part_ref[0:2, :] = jnp.dot(silu, mod_w_ref[0], preferred_element_type=F32)
+    part_ref[2:4, :] = jnp.dot(silu, mod_w_ref[1], preferred_element_type=F32)
+    part_ref[4:5, :] = jnp.dot(silu, mod_w_ref[2], preferred_element_type=F32)[0:1]
+    pl.semaphore_wait(barrier, 13)
     phase_x = [
         remote(part_ref, xbuf.at[n], send_sem.at[n], recv_sem.at[n], *peer) for n, peer in enumerate(xs)
     ]
     for copy in phase_x:
         copy.start()
-    loads[0].wait()
-    loads[1].wait()
+    for load in loads[5:7]:
+        load.wait()
 
     def norms(src_ref, base):
         def step(i, carry):
@@ -180,49 +202,54 @@
     ]
     for copy in phase_z:
         copy.start()
+    for load in loads[7:]:
+        load.wait()
     for copy in phase_z:
         copy.wait()
     whole = sum_ref[...] + zbuf[0] + zbuf[1] + zbuf[2]
     own_ref[...] = whole[0:4]
     gate_row_ref[...] = whole[4:5]
-    t = lax.axis_index("tp")
     phase_t = [
-        remote(own_ref, tbuf.at[t], send_sem.at[6 + n], recv_sem.at[6 + n], *peer) for n, peer in enumerate(ts)
+        remote(own_ref, tbuf.at[t], send_sem.at[6 + n], recv_sem.at[6 + n], "tp", peer)
+        for n, peer in enumerate(targets)
     ]
     for copy in phase_t:
         copy.start()
     tbuf[t] = own_ref[...]
-    pre_ref[...] = jnp.zeros_like(pre_ref)
+    wide = own_ref.shape[1]
+
+    def piece(n, block):
+        cols = pl.ds(pl.multiple_of(block * wide, wide), wide)
+        gain = gain_ref[:, cols]
+        rows = tbuf[block]
+        slot = n % 2
+        for src_ref, base, count, s in ((lat_ref, 0, n_lat, 0), (ctx_ref, n_lat, n_ctx, 1)):
+            a = gain * (1.0 + rows[2 + s : 3 + s, :])
+            b = rows[s : s + 1, :]
+            x = src_ref[:, cols].astype(F32)
+            inv = inv_ref[base : base + count, :]
+            y = [
+                x[:, j : j + TILE] * inv * a[:, j : j + TILE] + b[:, j : j + TILE] for j in range(0, wide, TILE)
+            ]
+            piece_ref[slot, base : base + count, :] = jnp.concatenate(y, axis=1).astype(BF16)
+        m = piece_ref[slot]
+        acc_ref[0] += jnp.dot(m, w_ref[0, cols, :], preferred_element_type=F32)
+        acc_ref[1] += jnp.dot(m, w_ref[1, cols, :], preferred_element_type=F32)
+        acc_ref[2, 0:n_lat] += jnp.dot(m[0:n_lat], w_ref[2, cols, :], preferred_element_type=F32)
+        pre_acc[0:n_all, 0:64] += mm_nt(m, wg_ref[:, cols])
+
+    piece(0, t)
+    for n, block in enumerate(sources):
+        phase_t[n].wait_recv()
+        piece(n + 1, block)
+    k_ref[...] = acc_ref[0].astype(BF16)
+    v_ref[...] = acc_ref[1].astype(BF16)
+    q_ref[...] = acc_ref[2, 0:n_lat].astype(BF16)
+    for j in range(0, n_lat + TILE, TILE):
+        rounded = pre_acc[j : j + TILE, :].astype(BF16).astype(F32)
+        pre_ref[:, j : j + TILE] = jnp.transpose(rounded)[0:64]
     for copy in phase_t:
-        copy.wait()
-    own_cols = own_ref.shape[1]
-    for n in range(8):
-        cols = slice(n * own_cols, (n + 1) * own_cols)
-        for s in range(2):
-            ab_ref[2 * s, :, cols] = gain_ref[:, cols] * (1.0 + tbuf[n, 2 + s : 3 + s, :])
-            ab_ref[2 * s + 1, :, cols] = tbuf[n, s : s + 1, :]
-
-    def scaled(src_ref, base, s):
-        def step(i, carry):
-            x = src_ref[pl.ds(i * 16, 16), :].astype(F32)
-            inv = inv_ref[pl.ds(base + i * 16, 16), 0:1]
-            y = x * inv * ab_ref[2 * s] + ab_ref[2 * s + 1]
-            mod_ref[pl.ds(base + i * 16, 16), :] = y.astype(BF16)
-            return carry
-
-        return step
-
-    lax.fori_loop(0, n_lat // 16, scaled(lat_ref, 0, 0), 0)
-    lax.fori_loop(0, n_ctx // 16, scaled(ctx_ref, n_lat, 1), 0)
-    for n, w in enumerate((ww_ref, wd_ref)):
-        r = slice(32 * n, 32 * n + 32)
-        pre_ref[r, 0:n_lat] = mm_nt(w[...], mod_ref[0:n_lat, :]).astype(BF16).astype(F32)
-        pre_ref[r, n_lat : n_lat + n_ctx] = mm_nt(w[...], mod_ref[n_lat:, :]).astype(BF16).astype(F32)
-    for load in loads[2:]:
-        load.wait()
-    k_ref[...] = mm(mod_ref[...], w_ref[0]).astype(BF16)
-    v_ref[...] = mm(mod_ref[...], w_ref[1]).astype(BF16)
-    q_ref[...] = mm(mod_ref[0:n_lat, :], w_ref[2]).astype(BF16)
+        copy.wait_send()
 
 
 def inverses(ad_ref, t_ref, base, count):
@@ -309,23 +336,6 @@
         sp = cols_ref[n_lat:, G + h : G + h + 1] - rows_ref[G + h : G + h + 1, n_lat:]
         dm = jnp.where(keep, jnp.exp(jnp.where(keep, sp, 0.0)), 0.0)
         ad_ref[4 * blocks + h] = (g2 * dm * cols_ref[n_lat:, RATE + h : RATE + h + 1]).astype(BF16)
-    inverses(ad_ref, t_ref, 4 * blocks, 2)
-    for h in range(2):
-        ci = kinv[h][n_lat:]
-        cr = slice(n_lat, n_lat + TILE)
-        rate = cols_ref[cr, RATE + h : RATE + h + 1]
-        eg = cols_ref[cr, EG + h : EG + h + 1]
-        late = cols_ref[cr, LATE + h : LATE + h + 1]
-        kc = kctx(h)
-        b = jnp.concatenate([vctx(h).astype(F32) * rate, kc.astype(F32) * (rate * eg * ci)], axis=1)
-        x = mm(t_ref[4 * blocks + h], b)
-        xl = (x * (late * ci)).astype(BF16)
-        for d in range(2):
-            c = d * 2 + h
-            m = mm_tn(kc[0:n_ctx], xl[d * n_ctx : (d + 1) * n_ctx])
-            diag = jnp.where(xor == 0, dec_ctx[c : c + 1, :], 0.0)
-            ctx_map[c] = jnp.concatenate([diag - m[:, TILE:], m[:, :TILE]], axis=1).astype(BF16)
-
     pl.semaphore_wait(barrier, 9)
 
     def to_row(base, maps, everyone):
@@ -347,8 +357,6 @@
             copy.start()
         everyone[z_at] = total[...]
         return copies
-
-    ctx_rows = to_row(0, ctx_map, ctx_all)
 
     qinvs = []
     for h in range(2):
@@ -381,15 +389,67 @@
                 p_ref[(c, *at)] = (qk_ref[(h, *at)] * dm).astype(BF16)
 
     def invert(part, carry):
-        inverses(ad_ref, t_ref, part * 8, 8)
+        inverses(ad_ref, t_ref, part * (tiles // 2), tiles // 2)
         return carry
 
-    lax.fori_loop(0, 4 * blocks // 8, invert, 0)
+    tiles = ad_ref.shape[0]
+    lax.fori_loop(0, 2, invert, 0)
+
+    for h in range(2):
+        ci = kinv[h][n_lat:]
+        cr = slice(n_lat, n_lat + TILE)
+        rate = cols_ref[cr, RATE + h : RATE + h + 1]
+        eg = cols_ref[cr, EG + h : EG + h + 1]
+        late = cols_ref[cr, LATE + h : LATE + h + 1]
+        kc = kctx(h)
+        b = jnp.concatenate([vctx(h).astype(F32) * rate, kc.astype(F32) * (rate * eg * ci)], axis=1)
+        x = mm(t_ref[4 * blocks + h], b)
+        xl = (x * (late * ci)).astype(BF16)
+        for d in range(2):
+            c = d * 2 + h
+            m = mm_tn(kc[0:n_ctx], xl[d * n_ctx : (d + 1) * n_ctx])
+            diag = jnp.where(xor == 0, dec_ctx[c : c + 1, :], 0.0)
+            ctx_map[c] = jnp.concatenate([diag - m[:, TILE:], m[:, :TILE]], axis=1).astype(BF16)
+
+    ctx_rows = to_row(0, ctx_map, ctx_all)
 
     backwards = x_at >= 2
 
     def place(n, size):
         return jnp.where(backwards, size - 1 - n, n)
+
+    lates, fronts, sides = {}, {}, {}
+    for n in range(blocks):
+        for c in range(4):
+            d, h = c // 2, c % 2
+            i = n if d == 0 else blocks - 1 - n
+            r = slice(i * TILE, (i + 1) * TILE)
+            rate = cols_ref[r, RATE + c : RATE + c + 1]
+            ki = kinv[h][r]
+            vi = v_ref[r, h * TILE : (h + 1) * TILE].astype(F32) * rate
+            wi = k_ref[r, h * TILE : (h + 1) * TILE].astype(F32) * (rate * cols_ref[r, EG + c : EG + c + 1] * ki)
+            lates[c, n] = cols_ref[r, LATE + c : LATE + c + 1] * ki
+            t = t_ref[c * blocks + i]
+            fronts[c, n] = mm(t, jnp.concatenate([vi, wi], axis=1))
+            if n > 0:
+                done = slice(0, i * TILE) if d == 0 else slice((i + 1) * TILE, n_lat)
+                sides[c, n] = mm(t, ao_ref[c, r, done]).astype(BF16)
+    for n in range(blocks):
+        for c in range(4):
+            d = c // 2
+            i = n if d == 0 else blocks - 1 - n
+            r = slice(i * TILE, (i + 1) * TILE)
+            x = fronts[c, n]
+            if n > 0:
+                done = slice(0, i * TILE) if d == 0 else slice((i + 1) * TILE, n_lat)
+                x = x - mm(sides[c, n], x_ref[c, done, :])
+            x_ref[c, r, :] = x.astype(BF16)
+            xl_ref[c, r, :] = (x * lates[c, n]).astype(BF16)
+    for c in range(4):
+        m = mm_tn(kcols(c % 2), xl_ref[c])
+        diag = jnp.where(xor == 0, dec_lat[c : c + 1, :], 0.0)
+        lat_map[c] = jnp.concatenate([diag - m[:, TILE:], m[:, :TILE]], axis=1).astype(BF16)
+    lat_rows = to_row(6, lat_map, lat_all)
 
     for copy in ctx_rows:
         copy.wait()
@@ -398,30 +458,6 @@
         total = then(ctx_all[place(n, 4)], total)
     ctx_total[...] = total.astype(BF16)
     ctx_columns = to_column(3, ctx_total, ctx_totals)
-
-    for c in range(4):
-        d, h = c // 2, c % 2
-        order = list(range(blocks)) if d == 0 else list(reversed(range(blocks)))
-        for n, i in enumerate(order):
-            r = slice(i * TILE, (i + 1) * TILE)
-            rate = cols_ref[r, RATE + c : RATE + c + 1]
-            eg = cols_ref[r, EG + c : EG + c + 1]
-            late = cols_ref[r, LATE + c : LATE + c + 1]
-            ki = kinv[h][r]
-            vi = v_ref[r, h * TILE : (h + 1) * TILE].astype(F32) * rate
-            wi = k_ref[r, h * TILE : (h + 1) * TILE].astype(F32) * (rate * eg * ki)
-            b = jnp.concatenate([vi, wi], axis=1)
-            if n > 0:
-                done = slice(0, i * TILE) if d == 0 else slice((i + 1) * TILE, n_lat)
-                b = b - mm(ao_ref[c, r, done], x_ref[c, done, :])
-            x = mm(t_ref[c * blocks + i], b)
-            x_ref[c, r, :] = x.astype(BF16)
-            xl_ref[c, r, :] = (x * (late * ki)).astype(BF16)
-    for c in range(4):
-        m = mm_tn(kcols(c % 2), xl_ref[c])
-        diag = jnp.where(xor == 0, dec_lat[c : c + 1, :], 0.0)
-        lat_map[c] = jnp.concatenate([diag - m[:, TILE:], m[:, :TILE]], axis=1).astype(BF16)
-    lat_rows = to_row(6, lat_map, lat_all)
 
     for h in range(2):
         o1 = []
@@ -439,6 +475,15 @@
                 else:
                     o1_ref[h, r, :] = o1[i] + ow[:, :TILE]
 
+    for copy in lat_rows:
+        copy.wait()
+    total = lat_all[place(0, 4)].astype(F32)
+    for n in range(1, 4):
+        at = place(n, 4)
+        prefix_ref[at] = total
+        total = then(lat_all[at], total)
+    lat_total[...] = total.astype(BF16)
+    lat_columns = to_column(9, lat_total, lat_totals)
     for copy in ctx_columns:
         copy.wait()
     state = None
@@ -446,17 +491,6 @@
         one = ctx_totals[place(n, 4)]
         off = one[:, TILE:].astype(F32)
         state = off if n == 0 else mul_precise(one[:, :TILE], state) + off
-    for copy in lat_rows:
-        copy.wait()
-    total = None
-    for n in range(4):
-        at = place(n, 4)
-        one = lat_all[at]
-        if n > 0:
-            prefix_ref[at] = total
-        total = one.astype(F32) if n == 0 else then(one, total)
-    lat_total[...] = total.astype(BF16)
-    lat_columns = to_column(9, lat_total, lat_totals)
     for copy in lat_columns:
         copy.wait()
     z_place = place(z_at, 4)
@@ -468,8 +502,7 @@
     for n in range(1, 4):
         at = place(n, 4)
         mk = prefix_ref[at]
-        hi, lo = split_rows(mk[:, :TILE])
-        start_ref[at] = (mul_precise(hi, state) + mm(lo, state) + mk[:, TILE:]).astype(BF16)
+        start_ref[at] = (mul_precise(mk[:, :TILE].astype(BF16), state) + mk[:, TILE:]).astype(BF16)
     starts = to_row(12, start_ref, mine_ref)
     for copy in starts:
         copy.wait()
@@ -554,7 +587,7 @@
     width = n_lat + TILE
     vm = pl.BlockSpec(memory_space=pltpu.VMEM)
     sm = pl.BlockSpec(memory_space=pltpu.SMEM)
-    hb = pl.BlockSpec(memory_space=pl.ANY)
+    hb = pl.BlockSpec(memory_space=pltpu.HBM)
     gates = [jnp.transpose(w, (1, 2, 0)).reshape(32, -1) for w in (write_weight, decay_weight)]
     shape = jax.ShapeDtypeStruct
     q, k, v, pre, gate_row = pl.pallas_call(
@@ -563,12 +596,15 @@
             shape((n_lat, pair), BF16), shape((n_all, pair), BF16), shape((n_all, pair), BF16),
             shape((64, width), F32), shape((1, own_cols), F32),
         ),
-        in_specs=[vm] * 8 + [hb] * 5,
+        in_specs=[hb] * 13,
         out_specs=(vm,) * 5,
         scratch_shapes=[
+            pltpu.VMEM(condition.shape, BF16), pltpu.VMEM(condition.shape, BF16),
+            pltpu.VMEM((3, *shift_weight.shape), BF16), pltpu.VMEM((1, d), F32), pltpu.VMEM((64, d), BF16),
             pltpu.VMEM((n_lat, d), BF16), pltpu.VMEM((n_ctx, d), BF16), pltpu.VMEM((3, d, pair), BF16),
-            pltpu.SemaphoreType.DMA((5,)), pltpu.VMEM((n_all, TILE), F32), pltpu.VMEM((4, 1, d), F32),
-            pltpu.VMEM((n_all, d), BF16), pltpu.VMEM((8, own_cols), F32), pltpu.VMEM((8, own_cols), F32),
+            pltpu.SemaphoreType.DMA((13,)), pltpu.VMEM((n_all, TILE), F32), pltpu.VMEM((2, n_all, own_cols), BF16),
+            pltpu.VMEM((3, n_all, pair), F32), pltpu.VMEM((width, TILE), F32),
+            pltpu.VMEM((8, own_cols), F32), pltpu.VMEM((8, own_cols), F32),
             pltpu.VMEM((4, own_cols), F32), pltpu.VMEM((3, 8, own_cols), F32), pltpu.VMEM((3, 8, own_cols), F32),
             pltpu.VMEM((8, 4, own_cols), F32), pltpu.SemaphoreType.DMA((13,)), pltpu.SemaphoreType.DMA((13,)),
         ],
@@ -577,7 +613,7 @@
         ),
         name="project",
     )(
-        condition.reshape(1, -1), context_condition.reshape(1, -1), shift_weight, scale_weight, gate_weight,
+        condition, context_condition, shift_weight, scale_weight, gate_weight,
         norm_gain.reshape(1, -1), *gates, latent, context, query_weight, key_weight, value_weight,
     )
     one_map = (TILE, 2 * TILE)

time: 82.4 us -> 73.6 us (0.89)
  Pallas kernels: 71.7 us -> 62.9 us
    pallas_call x1, Pallas kernels: 30.6 us -> 23 us  [body(): pl.pallas_call(project_kernel, out_shape=(shape((n_lat, pair), BF16), sha...]
    reshape x2 -> x0, local copies, waits for them, and re-layouts: 1.32 us -> none  [the longest x1 0.66 us: body(): condition.reshape(1, -1)]
    unnamed x27 -> x31, local copies, waits for them, and re-layouts: 8.91 us -> 10.2 us
    pallas_call x1, Pallas kernels: 41.1 us -> 39.8 us  [body(): pl.pallas_call(token_kernel, out_shape=shape((n_lat, own_cols), BF16), in...]
where the time goes in v2:
time: 73.6 us; the launch traced here: 73.2 us
  Pallas kernels  62.9 us (85%)
  local copies, waits for them, and re-layouts  10.2 us (14%)
    pallas_call x1, Pallas kernels, body(): pl.pallas_call(token_kernel, out_shape=shape((n_lat, own_cols), BF16), in...  39.8 us
    pallas_call x1, Pallas kernels, body(): pl.pallas_call(project_kernel, out_shape=(shape((n_lat, pair), BF16), sha...  23 us
    unnamed x31, local copies, waits for them, and re-layouts  10.2 us

profile of v2, /device:TPU:1, one launch (start us, length us, event | category | flops | bytes accessed | tf_op | source)
XLA Modules:
  0.0 73.2 jit_solution(17401005628356355003)
XLA Ops:
  0.0 0.0 copy-start
  0.0 1.6 %copy-done = bf16[4096,256]{1,0:T(8,128)(2,1)S(1)} copy-done((bf16[4096,256]{1,0:T(8,128)(2,1)S(1)}, bf16[4096,256]{1,0:T(8,128)(2,1)}, u32[]{:S(2)}) %copy-start) | copy-done | bytes 2097176
  1.6 0.0 copy-start.2
  1.6 1.0 %copy-done.2 = bf16[64,4096]{1,0:T(8,128)(2,1)S(1)} copy-done((bf16[64,4096]{1,0:T(8,128)(2,1)S(1)}, bf16[64,4096]{1,0:T(8,128)(2,1)}, u32[]{:S(2)}) %copy-start.2) | copy-done | bytes 524312
  2.6 0.0 copy-start.3
  2.6 0.9 %copy-done.3 = bf16[256,512]{1,0:T(8,128)(2,1)S(1)} copy-done((bf16[256,512]{1,0:T(8,128)(2,1)S(1)}, bf16[256,512]{1,0:T(8,128)(2,1)}, u32[]{:S(2)}) %copy-start.3) | copy-done | bytes 262168
  3.6 0.0 copy-start.4
  3.6 0.9 %copy-done.4 = bf16[256,512]{1,0:T(8,128)(2,1)S(1)} copy-done((bf16[256,512]{1,0:T(8,128)(2,1)S(1)}, bf16[256,512]{1,0:T(8,128)(2,1)}, u32[]{:S(2)}) %copy-start.4) | copy-done | bytes 262168
  4.5 0.0 copy-start.5
  4.5 0.9 %copy-done.5 = bf16[256,512]{1,0:T(8,128)(2,1)S(1)} copy-done((bf16[256,512]{1,0:T(8,128)(2,1)S(1)}, bf16[256,512]{1,0:T(8,128)(2,1)}, u32[]{:S(2)}) %copy-start.5) | copy-done | bytes 262168
  5.5 0.9 %copy-done.6 = bf16[4096,2,16]{0,2,1:T(8,128)(2,1)S(1)} copy-done((bf16[4096,2,16]{0,2,1:T(8,128)(2,1)S(1)}, bf16[4096,2,16]{0,2,1:T(8,128)(2,1)}, u32[]{:S(2)}) %copy-start.6) | copy-done | bytes 262168
  6.4 0.9 %copy-done.7 = bf16[4096,2,16]{0,2,1:T(8,128)(2,1)S(1)} copy-done((bf16[4096,2,16]{0,2,1:T(8,128)(2,1)S(1)}, bf16[4096,2,16]{0,2,1:T(8,128)(2,1)}, u32[]{:S(2)}) %copy-start.7) | copy-done | bytes 262168
  7.4 0.7 copy-done.8
  8.1 0.7 copy-done.12
  8.8 0.7 copy-done.13
  9.4 0.0 copy-start.14
  9.4 23.0 %project.1 = (bf16[512,256]{1,0:T(8,128)(2,1)S(1)}, bf16[576,256]{1,0:T(8,128)(2,1)S(1)}, bf16[576,256]{1,0:T(8,128)(2,1)S(1)}, f32[64,640]{1,0:T(8,128)S(1)}, f32[1,512]{1,0:T(1,128)S(1)}) custom-call(bf16[256]{0:T(256)(128)(2,1)S(1)} %copy-done.12, bf16[256]{0:T(256)(128)(2,1)S(1)} %copy-done.13, bf16[256,512]{1,0:T(8,128)(2,1)S(1)} %copy-done.3, ...), custom_call_target="tpu_custom_call" | custom-call | tf_op jit(solution)/shard_map/project/pallas_call | solution.py:593
  32.5 0.0 copy-done.1
  32.5 0.0 copy-done.9
  32.5 0.0 copy-done.10
  32.5 0.0 copy-done.11
  32.5 0.0 copy-done.14
  32.5 39.8 %tokens.1 = bf16[512,512]{1,0:T(8,128)(2,1)S(1)} custom-call(bf16[512,256]{1,0:T(8,128)(2,1)S(1)} %get-tuple-element.10.q_ref, bf16[576,256]{1,0:T(8,128)(2,1)S(1)} %get-tuple-element.11.k_ref, bf16[576,256]{1,0:T(8,128)(2,1)S(1)} %get-tuple-element.12.v_ref, f32[64,640]{1,0:T(8,128)S(1)} %get-tuple-element.13.pre_ref, ...), custom_call_target="tpu_custom_call" | custom-call | tf_op jit(solution)/shard_map/tokens/pallas_call | solution.py:620
  72.4 0.8 %copy.20 = bf16[512,512]{1,0:T(8,128)(2,1)} copy(bf16[512,512]{1,0:T(8,128)(2,1)S(1)} %tokens.1) | data formatting | bytes 1048576
  (9 shorter events, 0.0 us)
Async XLA Ops:
  0.0 1.6 %copy-start = (bf16[4096,256]{1,0:T(8,128)(2,1)S(1)}, bf16[4096,256]{1,0:T(8,128)(2,1)}, u32[]{:S(2)}) copy-start(bf16[4096,256]{1,0:T(8,128)(2,1)} %wq_hbm.1) | copy-start | bytes 6291460
  1.6 1.0 %copy-start.2 = (bf16[64,4096]{1,0:T(8,128)(2,1)S(1)}, bf16[64,4096]{1,0:T(8,128)(2,1)}, u32[]{:S(2)}) copy-start(bf16[64,4096]{1,0:T(8,128)(2,1)} %ctx_hbm.1) | copy-start | bytes 1572868
  2.6 0.9 %copy-start.3 = (bf16[256,512]{1,0:T(8,128)(2,1)S(1)}, bf16[256,512]{1,0:T(8,128)(2,1)}, u32[]{:S(2)}) copy-start(bf16[256,512]{1,0:T(8,128)(2,1)} %shift_hbm.1) | copy-start | bytes 786436
  3.6 0.9 %copy-start.4 = (bf16[256,512]{1,0:T(8,128)(2,1)S(1)}, bf16[256,512]{1,0:T(8,128)(2,1)}, u32[]{:S(2)}) copy-start(bf16[256,512]{1,0:T(8,128)(2,1)} %scale_hbm.1) | copy-start | bytes 786436
  4.5 0.9 %copy-start.5 = (bf16[256,512]{1,0:T(8,128)(2,1)S(1)}, bf16[256,512]{1,0:T(8,128)(2,1)}, u32[]{:S(2)}) copy-start(bf16[256,512]{1,0:T(8,128)(2,1)} %gate_hbm.1) | copy-start | bytes 786436
  5.5 0.9 %copy-start.6 = (bf16[4096,2,16]{0,2,1:T(8,128)(2,1)S(1)}, bf16[4096,2,16]{0,2,1:T(8,128)(2,1)}, u32[]{:S(2)}) copy-start(bf16[4096,2,16]{0,2,1:T(8,128)(2,1)} %param.29) | copy-start | bytes 786436
  6.4 0.9 %copy-start.7 = (bf16[4096,2,16]{0,2,1:T(8,128)(2,1)S(1)}, bf16[4096,2,16]{0,2,1:T(8,128)(2,1)}, u32[]{:S(2)}) copy-start(bf16[4096,2,16]{0,2,1:T(8,128)(2,1)} %param.30) | copy-start | bytes 786436
  7.4 0.7 copy-start.8
  8.1 0.7 copy-start.12
  8.8 0.7 copy-start.13
  9.4 23.1 %copy-start.1 = (bf16[2048,512]{1,0:T(8,128)(2,1)S(1)}, bf16[2048,512]{1,0:T(8,128)(2,1)}, u32[]{:S(2)}) copy-start(bf16[2048,512]{1,0:T(8,128)(2,1)} %ow_hbm.1) | copy-start | bytes 6291460
  9.4 23.1 %copy-start.9 = (f32[2,16]{1,0:T(2,128)S(1)}, f32[2,16]{1,0:T(2,128)}, u32[]{:S(2)}) copy-start(f32[2,16]{1,0:T(2,128)} %wb_ref.1) | copy-start | bytes 388
  9.4 23.1 %copy-start.10 = (f32[2,16]{1,0:T(2,128)S(1)}, f32[2,16]{1,0:T(2,128)}, u32[]{:S(2)}) copy-start(f32[2,16]{1,0:T(2,128)} %db_ref.1) | copy-start | bytes 388
  9.4 23.1 %copy-start.11 = (f32[2,16]{1,0:T(2,128)S(1)}, f32[2,16]{1,0:T(2,128)}, u32[]{:S(2)}) copy-start(f32[2,16]{1,0:T(2,128)} %lr_ref.1) | copy-start | bytes 388
  9.4 23.1 %copy-start.14 = (f32[128]{0:T(128)S(1)}, f32[128]{0:T(128)}, u32[]{:S(2)}) copy-start(f32[128]{0:T(128)} %param.34) | copy-start | bytes 1540

commit v3 on v2

--- a/solution.py
+++ b/solution.py
@@ -12,6 +12,7 @@
 F32 = jnp.float32
 BF16 = jnp.bfloat16
 TILE = 128
+VMEM_LIMIT = 67043328
 MESH = pl.DeviceIdType.MESH
 LEVELS = (1, 2, 3, 4, 5, 6)
 
@@ -125,133 +126,6 @@
     return [(axis, lax.rem(me + k, size)) for k in range(1, size)]
 
 
-def project_kernel(
-    cond_hbm, cctx_hbm, shift_hbm, scale_hbm, gate_hbm, gain_hbm, ww_hbm, wd_hbm,
-    lat_hbm, ctx_hbm, wq_hbm, wk_hbm, wv_hbm,
-    q_ref, k_ref, v_ref, pre_ref, gate_row_ref,
-    cond_ref, cctx_ref, mod_w_ref, gain_ref, wg_ref, lat_ref, ctx_ref, w_ref, load_sem,
-    inv_ref, piece_ref, acc_ref, pre_acc,
-    part_ref, sum_ref, own_ref, xbuf, zbuf, tbuf, send_sem, recv_sem,
-):
-    barrier = pltpu.get_barrier_semaphore()
-    t = lax.axis_index("tp")
-    y_at, core = t // 2, lax.rem(t, 2)
-    up = lax.rem(y_at + 1, 4) * 2 + core
-    down = lax.rem(y_at + 3, 4) * 2 + core
-    across = lax.rem(y_at + 2, 4) * 2 + core
-
-    def other(block):
-        return block + 1 - 2 * core
-
-    targets = [other(t), up, down, other(up), other(down), across, other(across)]
-    sources = [other(t), down, up, other(down), other(up), across, other(across)]
-    xs, zs = ring_peers("sp_1", 4), ring_peers("sp_0", 4)
-    greet(barrier, xs + zs + [("tp", peer) for peer in targets])
-    loads = [
-        pltpu.make_async_copy(src, dst, load_sem.at[n])
-        for n, (src, dst) in enumerate(
-            (
-                (cond_hbm, cond_ref), (cctx_hbm, cctx_ref), (shift_hbm, mod_w_ref.at[0]), (scale_hbm, mod_w_ref.at[1]),
-                (gate_hbm, mod_w_ref.at[2]), (lat_hbm, lat_ref), (ctx_hbm, ctx_ref), (gain_hbm, gain_ref),
-                (ww_hbm, wg_ref.at[0:32]), (wd_hbm, wg_ref.at[32:64]),
-                (wk_hbm, w_ref.at[0]), (wv_hbm, w_ref.at[1]), (wq_hbm, w_ref.at[2]),
-            )
-        )
-    ]
-    for load in loads:
-        load.start()
-    n_lat, n_ctx = lat_ref.shape[0], ctx_ref.shape[0]
-    n_all = n_lat + n_ctx
-    acc_ref[...] = jnp.zeros_like(acc_ref)
-    pre_acc[...] = jnp.zeros_like(pre_acc)
-    part_ref[...] = jnp.zeros_like(part_ref)
-    for load in loads[:5]:
-        load.wait()
-    u = jnp.concatenate(
-        [cond_ref[...].astype(F32).reshape(1, -1), cctx_ref[...].astype(F32).reshape(1, -1)], axis=0
-    )
-    silu = (u / (1.0 + jnp.exp(-u))).astype(BF16)
-    part_ref[0:2, :] = jnp.dot(silu, mod_w_ref[0], preferred_element_type=F32)
-    part_ref[2:4, :] = jnp.dot(silu, mod_w_ref[1], preferred_element_type=F32)
-    part_ref[4:5, :] = jnp.dot(silu, mod_w_ref[2], preferred_element_type=F32)[0:1]
-    pl.semaphore_wait(barrier, 13)
-    phase_x = [
-        remote(part_ref, xbuf.at[n], send_sem.at[n], recv_sem.at[n], *peer) for n, peer in enumerate(xs)
-    ]
-    for copy in phase_x:
-        copy.start()
-    for load in loads[5:7]:
-        load.wait()
-
-    def norms(src_ref, base):
-        def step(i, carry):
-            x = src_ref[pl.ds(i * 16, 16), :].astype(F32)
-            inv = lax.rsqrt(jnp.mean(x * x, axis=-1, keepdims=True) + EPS)
-            inv_ref[pl.ds(base + i * 16, 16), :] = jnp.broadcast_to(inv, (16, TILE))
-            return carry
-
-        return step
-
-    lax.fori_loop(0, n_lat // 16, norms(lat_ref, 0), 0)
-    lax.fori_loop(0, n_ctx // 16, norms(ctx_ref, n_lat), 0)
-    for copy in phase_x:
-        copy.wait()
-    sum_ref[...] = part_ref[...] + xbuf[0] + xbuf[1] + xbuf[2]
-    phase_z = [
-        remote(sum_ref, zbuf.at[n], send_sem.at[3 + n], recv_sem.at[3 + n], *peer) for n, peer in enumerate(zs)
-    ]
-    for copy in phase_z:
-        copy.start()
-    for load in loads[7:]:
-        load.wait()
-    for copy in phase_z:
-        copy.wait()
-    whole = sum_ref[...] + zbuf[0] + zbuf[1] + zbuf[2]
-    own_ref[...] = whole[0:4]
-    gate_row_ref[...] = whole[4:5]
-    phase_t = [
-        remote(own_ref, tbuf.at[t], send_sem.at[6 + n], recv_sem.at[6 + n], "tp", peer)
-        for n, peer in enumerate(targets)
-    ]
-    for copy in phase_t:
-        copy.start()
-    tbuf[t] = own_ref[...]
-    wide = own_ref.shape[1]
-
-    def piece(n, block):
-        cols = pl.ds(pl.multiple_of(block * wide, wide), wide)
-        gain = gain_ref[:, cols]
-        rows = tbuf[block]
-        slot = n % 2
-        for src_ref, base, count, s in ((lat_ref, 0, n_lat, 0), (ctx_ref, n_lat, n_ctx, 1)):
-            a = gain * (1.0 + rows[2 + s : 3 + s, :])
-            b = rows[s : s + 1, :]
-            x = src_ref[:, cols].astype(F32)
-            inv = inv_ref[base : base + count, :]
-            y = [
-                x[:, j : j + TILE] * inv * a[:, j : j + TILE] + b[:, j : j + TILE] for j in range(0, wide, TILE)
-            ]
-            piece_ref[slot, base : base + count, :] = jnp.concatenate(y, axis=1).astype(BF16)
-        m = piece_ref[slot]
-        acc_ref[0] += jnp.dot(m, w_ref[0, cols, :], preferred_element_type=F32)
-        acc_ref[1] += jnp.dot(m, w_ref[1, cols, :], preferred_element_type=F32)
-        acc_ref[2, 0:n_lat] += jnp.dot(m[0:n_lat], w_ref[2, cols, :], preferred_element_type=F32)
-        pre_acc[0:n_all, 0:64] += mm_nt(m, wg_ref[:, cols])
-
-    piece(0, t)
-    for n, block in enumerate(sources):
-        phase_t[n].wait_recv()
-        piece(n + 1, block)
-    k_ref[...] = acc_ref[0].astype(BF16)
-    v_ref[...] = acc_ref[1].astype(BF16)
-    q_ref[...] = acc_ref[2, 0:n_lat].astype(BF16)
-    for j in range(0, n_lat + TILE, TILE):
-        rounded = pre_acc[j : j + TILE, :].astype(BF16).astype(F32)
-        pre_ref[:, j : j + TILE] = jnp.transpose(rounded)[0:64]
-    for copy in phase_t:
-        copy.wait_send()
-
-
 def inverses(ad_ref, t_ref, base, count):
     xor = iota2((TILE, TILE), 0) ^ iota2((TILE, TILE), 1)
     eye = jnp.where(xor == 0, 1.0, 0.0)
@@ -269,11 +143,10 @@
         t_ref[base + n] = ts[n]
 
 
-def token_kernel(
-    q_ref, k_ref, v_ref, pre_ref, gate_row_ref, gain_ref, wb_ref, db_ref, lr_ref, lat_hbm, ow_hbm,
+def mix_tokens(
+    q_ref, k_ref, v_ref, pre_ref, gate_row_ref, gain_ref, wb_ref, db_ref, lr_ref, lat_ref, ow_ref,
     out_ref,
-    ow_ref, res_ref, load_sem,
-    rows_ref, cols_ref, gk_ref, qk_ref, ad_ref, t_ref, ao_ref, p_ref, x_ref, xl_ref, o1_ref, q2_ref,
+    rows_ref, cols_ref, gk_ref, qk_ref, dm_ref, ad_ref, t_ref, ao_ref, p_ref, x_ref, xl_ref, o1_ref, q2_ref,
     lat_map, ctx_map, lat_all, ctx_all, prefix_ref, lat_total, ctx_total, lat_totals, ctx_totals,
     start_ref, mine_ref, ho_ref, send_sem, recv_sem, ho_send, ho_recv,
 ):
@@ -287,16 +160,8 @@
     down = lax.rem(y_at + 3, 4) * 2 + core
     across = lax.rem(y_at + 2, 4) * 2 + core
     mate = y_at * 2 + 1 - core
-    barrier = pltpu.get_barrier_semaphore()
     xs, zs = ring_peers("sp_1", 4), ring_peers("sp_0", 4)
-    greet(barrier, xs + zs + [("tp", up), ("tp", down), ("tp", mate)])
     own_cols = out_ref.shape[1]
-    load_w = pltpu.make_async_copy(ow_hbm, ow_ref, load_sem.at[0])
-    load_r = pltpu.make_async_copy(
-        lat_hbm.at[:, pl.ds(pl.multiple_of(t_at * own_cols, own_cols), own_cols)], res_ref, load_sem.at[1]
-    )
-    load_w.start()
-    load_r.start()
 
     dec_lat, dec_ctx = gate_rows(t_at * 2, pre_ref, wb_ref, db_ref, lr_ref, rows_ref, n_lat, n_ctx)
     for b in range(blocks + 1):
@@ -336,8 +201,6 @@
         sp = cols_ref[n_lat:, G + h : G + h + 1] - rows_ref[G + h : G + h + 1, n_lat:]
         dm = jnp.where(keep, jnp.exp(jnp.where(keep, sp, 0.0)), 0.0)
         ad_ref[4 * blocks + h] = (g2 * dm * cols_ref[n_lat:, RATE + h : RATE + h + 1]).astype(BF16)
-    pl.semaphore_wait(barrier, 9)
-
     def to_row(base, maps, everyone):
         copies = [
             remote(maps.at[peer], everyone.at[x_at], send_sem.at[base + n], recv_sem.at[base + n], axis, peer)
@@ -358,14 +221,9 @@
         everyone[z_at] = total[...]
         return copies
 
-    qinvs = []
     for h in range(2):
-        qh = q_ref[0:n_lat, h * TILE : (h + 1) * TILE]
-        qinv = inv_norm(qh) * (HEAD_DIM**-0.5)
-        qinvs.append(qinv)
         krow = rows_ref[KINV + h : KINV + h + 1, 0:n_lat]
         gk_ref[h] = mm_nt(kcols(h), kcols(h)) * kinv[h][0:n_lat] * krow
-        qk_ref[h] = mm_nt(qh, kcols(h)) * qinv * krow
     for c in range(4):
         d, h = c // 2, c % 2
         for i in range(blocks):
@@ -386,15 +244,9 @@
                     ad_ref[c * blocks + i] = jnp.where(ii == jj, 0.0, a).astype(BF16)
                 else:
                     ao_ref[(c, *at)] = a.astype(BF16)
-                p_ref[(c, *at)] = (qk_ref[(h, *at)] * dm).astype(BF16)
-
-    def invert(part, carry):
-        inverses(ad_ref, t_ref, part * (tiles // 2), tiles // 2)
-        return carry
-
-    tiles = ad_ref.shape[0]
-    lax.fori_loop(0, 2, invert, 0)
-
+                dm_ref[(c, *at)] = dm
+
+    inverses(ad_ref, t_ref, 0, ad_ref.shape[0])
     for h in range(2):
         ci = kinv[h][n_lat:]
         cr = slice(n_lat, n_lat + TILE)
@@ -459,6 +311,18 @@
     ctx_total[...] = total.astype(BF16)
     ctx_columns = to_column(3, ctx_total, ctx_totals)
 
+    qinvs = []
+    for h in range(2):
+        qh = q_ref[0:n_lat, h * TILE : (h + 1) * TILE]
+        qinv = inv_norm(qh) * (HEAD_DIM**-0.5)
+        qinvs.append(qinv)
+        qk_ref[h] = mm_nt(qh, kcols(h)) * qinv * rows_ref[KINV + h : KINV + h + 1, 0:n_lat]
+    for c in range(4):
+        d, h = c // 2, c % 2
+        for i in range(blocks):
+            r = slice(i * TILE, (i + 1) * TILE)
+            seen = slice(0, (i + 1) * TILE) if d == 0 else slice(i * TILE, n_lat)
+            p_ref[c, r, seen] = (qk_ref[h, r, seen] * dm_ref[c, r, seen]).astype(BF16)
     for h in range(2):
         o1 = []
         for d in range(2):
@@ -531,8 +395,6 @@
     hands[1] = hand(1, t_at, B, up)
     hands[2] = hand(2, t_at, A, down)
     hands[5] = hand(5, t_at, B, mate)
-    load_w.wait()
-    load_r.wait()
     depth = 2 * TILE
 
     def add(block):
@@ -567,9 +429,143 @@
     hands[12].wait_recv()
     hands[13].wait_recv()
     acc = acc + add(other(across))
-    out_ref[...] = (res_ref[...].astype(F32) + gate_row_ref[...] * acc).astype(BF16)
+    own = lat_ref[:, pl.ds(pl.multiple_of(t_at * own_cols, own_cols), own_cols)]
+    out_ref[...] = (own.astype(F32) + gate_row_ref[...] * acc).astype(BF16)
     for n in range(14):
         hands[n].wait_send()
+
+
+def mixer_kernel(
+    cond_hbm, cctx_hbm, shift_hbm, scale_hbm, gate_hbm, gain_hbm, ww_hbm, wd_hbm,
+    lat_hbm, ctx_hbm, wq_hbm, wk_hbm, wv_hbm, wb_hbm, db_hbm, lr_hbm, hg_hbm, ow_hbm,
+    out_ref,
+    q_ref, k_ref, v_ref, pre_ref, gate_row_ref,
+    cond_ref, cctx_ref, mod_w_ref, gain_ref, wg_ref, lat_ref, ctx_ref, w_ref, wb_ref, db_ref, lr_ref, hg_ref, ow_ref,
+    load_sem, inv_ref, piece_ref, acc_ref, pre_acc,
+    part_ref, sum_ref, own_ref, xbuf, zbuf, tbuf, mod_send, mod_recv, *scratch,
+):
+    barrier = pltpu.get_barrier_semaphore()
+    t = lax.axis_index("tp")
+    y_at, core = t // 2, lax.rem(t, 2)
+    up = lax.rem(y_at + 1, 4) * 2 + core
+    down = lax.rem(y_at + 3, 4) * 2 + core
+    across = lax.rem(y_at + 2, 4) * 2 + core
+
+    def other(block):
+        return block + 1 - 2 * core
+
+    targets = [other(t), up, down, other(up), other(down), across, other(across)]
+    sources = [other(t), down, up, other(down), other(up), across, other(across)]
+    xs, zs = ring_peers("sp_1", 4), ring_peers("sp_0", 4)
+    greet(barrier, xs + zs + [("tp", peer) for peer in targets])
+    loads = [
+        pltpu.make_async_copy(src, dst, load_sem.at[n])
+        for n, (src, dst) in enumerate(
+            (
+                (cond_hbm, cond_ref), (cctx_hbm, cctx_ref), (shift_hbm, mod_w_ref.at[0]), (scale_hbm, mod_w_ref.at[1]),
+                (gate_hbm, mod_w_ref.at[2]), (lat_hbm, lat_ref), (ctx_hbm, ctx_ref), (gain_hbm, gain_ref),
+                (ww_hbm, wg_ref.at[0:32]), (wd_hbm, wg_ref.at[32:64]),
+                (wk_hbm, w_ref.at[0]), (wv_hbm, w_ref.at[1]), (wq_hbm, w_ref.at[2]),
+                (wb_hbm, wb_ref), (db_hbm, db_ref), (lr_hbm, lr_ref), (hg_hbm, hg_ref), (ow_hbm, ow_ref),
+            )
+        )
+    ]
+    for load in loads:
+        load.start()
+    n_lat, n_ctx = lat_ref.shape[0], ctx_ref.shape[0]
+    n_all = n_lat + n_ctx
+    acc_ref[...] = jnp.zeros_like(acc_ref)
+    pre_acc[...] = jnp.zeros_like(pre_acc)
+    part_ref[...] = jnp.zeros_like(part_ref)
+    for load in loads[:5]:
+        load.wait()
+    u = jnp.concatenate(
+        [cond_ref[...].astype(F32).reshape(1, -1), cctx_ref[...].astype(F32).reshape(1, -1)], axis=0
+    )
+    silu = (u / (1.0 + jnp.exp(-u))).astype(BF16)
+    part_ref[0:2, :] = jnp.dot(silu, mod_w_ref[0], preferred_element_type=F32)
+    part_ref[2:4, :] = jnp.dot(silu, mod_w_ref[1], preferred_element_type=F32)
+    part_ref[4:5, :] = jnp.dot(silu, mod_w_ref[2], preferred_element_type=F32)[0:1]
+    pl.semaphore_wait(barrier, 13)
+    phase_x = [
+        remote(part_ref, xbuf.at[n], mod_send.at[n], mod_recv.at[n], *peer) for n, peer in enumerate(xs)
+    ]
+    for copy in phase_x:
+        copy.start()
+    for load in loads[5:7]:
+        load.wait()
+
+    def norms(src_ref, base):
+        def step(i, carry):
+            for j in range(4):
+                x = src_ref[pl.ds(i * 64 + j * 16, 16), :].astype(F32)
+                inv = lax.rsqrt(jnp.mean(x * x, axis=-1, keepdims=True) + EPS)
+                inv_ref[pl.ds(base + i * 64 + j * 16, 16), :] = jnp.broadcast_to(inv, (16, TILE))
+            return carry
+
+        return step
+
+    lax.fori_loop(0, n_lat // 64, norms(lat_ref, 0), 0)
+    lax.fori_loop(0, n_ctx // 64, norms(ctx_ref, n_lat), 0)
+    for copy in phase_x:
+        copy.wait()
+    sum_ref[...] = part_ref[...] + xbuf[0] + xbuf[1] + xbuf[2]
+    phase_z = [
+        remote(sum_ref, zbuf.at[n], mod_send.at[3 + n], mod_recv.at[3 + n], *peer) for n, peer in enumerate(zs)
+    ]
+    for copy in phase_z:
+        copy.start()
+    for load in loads[7:]:
+        load.wait()
+    for copy in phase_z:
+        copy.wait()
+    whole = sum_ref[...] + zbuf[0] + zbuf[1] + zbuf[2]
+    own_ref[...] = whole[0:4]
+    gate_row_ref[...] = whole[4:5]
+    phase_t = [
+        remote(own_ref, tbuf.at[t], mod_send.at[6 + n], mod_recv.at[6 + n], "tp", peer)
+        for n, peer in enumerate(targets)
+    ]
+    for copy in phase_t:
+        copy.start()
+    tbuf[t] = own_ref[...]
+    wide = own_ref.shape[1]
+
+    def piece(n, block):
+        cols = pl.ds(pl.multiple_of(block * wide, wide), wide)
+        gain = gain_ref[:, cols]
+        rows = tbuf[block]
+        slot = n % 2
+        for src_ref, base, count, s in ((lat_ref, 0, n_lat, 0), (ctx_ref, n_lat, n_ctx, 1)):
+            a = gain * (1.0 + rows[2 + s : 3 + s, :])
+            b = rows[s : s + 1, :]
+            x = src_ref[:, cols].astype(F32)
+            inv = inv_ref[base : base + count, :]
+            y = [
+                x[:, j : j + TILE] * inv * a[:, j : j + TILE] + b[:, j : j + TILE] for j in range(0, wide, TILE)
+            ]
+            piece_ref[slot, base : base + count, :] = jnp.concatenate(y, axis=1).astype(BF16)
+        m = piece_ref[slot]
+        acc_ref[0] += jnp.dot(m, w_ref[0, cols, :], preferred_element_type=F32)
+        acc_ref[1] += jnp.dot(m, w_ref[1, cols, :], preferred_element_type=F32)
+        acc_ref[2, 0:n_lat] += jnp.dot(m[0:n_lat], w_ref[2, cols, :], preferred_element_type=F32)
+        pre_acc[0:n_all, 0:64] += mm_nt(m, wg_ref[:, cols])
+
+    piece(0, t)
+    for n, block in enumerate(sources):
+        phase_t[n].wait_recv()
+        piece(n + 1, block)
+    k_ref[...] = acc_ref[0].astype(BF16)
+    v_ref[...] = acc_ref[1].astype(BF16)
+    q_ref[...] = acc_ref[2, 0:n_lat].astype(BF16)
+    for j in range(0, n_lat + TILE, TILE):
+        rounded = pre_acc[j : j + TILE, :].astype(BF16).astype(F32)
+        pre_ref[:, j : j + TILE] = jnp.transpose(rounded)[0:64]
+    mix_tokens(
+        q_ref, k_ref, v_ref, pre_ref, gate_row_ref, hg_ref, wb_ref, db_ref, lr_ref, lat_ref, ow_ref, out_ref, *scratch
+    )
+    for copy in phase_t:
+        copy.wait_send()
 
 
 def body(
@@ -586,46 +582,31 @@
     tiles = 4 * blocks + 2
     width = n_lat + TILE
     vm = pl.BlockSpec(memory_space=pltpu.VMEM)
-    sm = pl.BlockSpec(memory_space=pltpu.SMEM)
     hb = pl.BlockSpec(memory_space=pltpu.HBM)
     gates = [jnp.transpose(w, (1, 2, 0)).reshape(32, -1) for w in (write_weight, decay_weight)]
     shape = jax.ShapeDtypeStruct
-    q, k, v, pre, gate_row = pl.pallas_call(
-        project_kernel,
-        out_shape=(
-            shape((n_lat, pair), BF16), shape((n_all, pair), BF16), shape((n_all, pair), BF16),
-            shape((64, width), F32), shape((1, own_cols), F32),
-        ),
-        in_specs=[hb] * 13,
-        out_specs=(vm,) * 5,
+    one_map = (TILE, 2 * TILE)
+    small = write_bias.shape
+    return pl.pallas_call(
+        mixer_kernel,
+        out_shape=shape((n_lat, own_cols), BF16),
+        in_specs=[hb] * 18,
+        out_specs=vm,
         scratch_shapes=[
+            pltpu.VMEM((n_lat, pair), BF16), pltpu.VMEM((n_all, pair), BF16), pltpu.VMEM((n_all, pair), BF16),
+            pltpu.VMEM((64, width), F32), pltpu.VMEM((1, own_cols), F32),
             pltpu.VMEM(condition.shape, BF16), pltpu.VMEM(condition.shape, BF16),
             pltpu.VMEM((3, *shift_weight.shape), BF16), pltpu.VMEM((1, d), F32), pltpu.VMEM((64, d), BF16),
             pltpu.VMEM((n_lat, d), BF16), pltpu.VMEM((n_ctx, d), BF16), pltpu.VMEM((3, d, pair), BF16),
-            pltpu.SemaphoreType.DMA((13,)), pltpu.VMEM((n_all, TILE), F32), pltpu.VMEM((2, n_all, own_cols), BF16),
+            pltpu.SMEM(small, F32), pltpu.SMEM(small, F32), pltpu.SMEM(small, F32), pltpu.VMEM((1, TILE), F32),
+            pltpu.VMEM(out_weight.shape, BF16), pltpu.SemaphoreType.DMA((18,)),
+            pltpu.VMEM((n_all, TILE), F32), pltpu.VMEM((2, n_all, own_cols), BF16),
             pltpu.VMEM((3, n_all, pair), F32), pltpu.VMEM((width, TILE), F32),
             pltpu.VMEM((8, own_cols), F32), pltpu.VMEM((8, own_cols), F32),
             pltpu.VMEM((4, own_cols), F32), pltpu.VMEM((3, 8, own_cols), F32), pltpu.VMEM((3, 8, own_cols), F32),
             pltpu.VMEM((8, 4, own_cols), F32), pltpu.SemaphoreType.DMA((13,)), pltpu.SemaphoreType.DMA((13,)),
-        ],
-        compiler_params=pltpu.CompilerParams(
-            collective_id=0, has_side_effects=True, vmem_limit_bytes=48 * 1024 * 1024
-        ),
-        name="project",
-    )(
-        condition, context_condition, shift_weight, scale_weight, gate_weight,
-        norm_gain.reshape(1, -1), *gates, latent, context, query_weight, key_weight, value_weight,
-    )
-    one_map = (TILE, 2 * TILE)
-    return pl.pallas_call(
-        token_kernel,
-        out_shape=shape((n_lat, own_cols), BF16),
-        in_specs=[vm] * 6 + [sm] * 3 + [hb] * 2,
-        out_specs=vm,
-        scratch_shapes=[
-            pltpu.VMEM(out_weight.shape, BF16), pltpu.VMEM((n_lat, own_cols), BF16), pltpu.SemaphoreType.DMA((2,)),
             pltpu.VMEM((TILE, width), F32), pltpu.VMEM((width, TILE), F32),
-            pltpu.VMEM((2, n_lat, n_lat), F32), pltpu.VMEM((2, n_lat, n_lat), F32),
+            pltpu.VMEM((2, n_lat, n_lat), F32), pltpu.VMEM((2, n_lat, n_lat), F32), pltpu.VMEM((4, n_lat, n_lat), F32),
             pltpu.VMEM((tiles, TILE, TILE), BF16), pltpu.VMEM((tiles, TILE, TILE), BF16),
             pltpu.VMEM((4, n_lat, n_lat), BF16), pltpu.VMEM((4, n_lat, n_lat), BF16),
             pltpu.VMEM((4, n_lat, 2 * TILE), BF16), pltpu.VMEM((4, n_lat, 2 * TILE), BF16),
@@ -640,10 +621,14 @@
             pltpu.SemaphoreType.DMA((14,)), pltpu.SemaphoreType.DMA((14,)),
         ],
         compiler_params=pltpu.CompilerParams(
-            collective_id=1, has_side_effects=True, vmem_limit_bytes=48 * 1024 * 1024
+            collective_id=0, has_side_effects=True, vmem_limit_bytes=VMEM_LIMIT
         ),
-        name="tokens",
-    )(q, k, v, pre, gate_row, head_gain.reshape(1, -1), write_bias, decay_bias, log_rate, latent, out_weight)
+        name="mixer",
+    )(
+        condition, context_condition, shift_weight, scale_weight, gate_weight, norm_gain.reshape(1, -1), *gates,
+        latent, context, query_weight, key_weight, value_weight, write_bias, decay_bias, log_rate,
+        head_gain.reshape(1, -1), out_weight,
+    )
 
 
 def solution(mesh):

time: 73.6 us -> 61.3 us (0.83)
  local copies, waits for them, and re-layouts: 10.2 us -> 1.87 us
  Pallas kernels: 62.9 us -> 59.3 us
    unnamed x31 -> x1, local copies, waits for them, and re-layouts: 10.2 us -> 1.87 us
    pallas_call x2 -> x1, Pallas kernels: 62.9 us -> 59.3 us  [body(): pl.pallas_call(mixer_kernel, out_shape=shape((n_lat, own_cols), BF16), in...]
where the time goes in v3:
time: 61.3 us; the launch traced here: 61.1 us
  Pallas kernels  59.3 us (97%)
  local copies, waits for them, and re-layouts  1.87 us (3%)
    pallas_call x1, Pallas kernels, body(): pl.pallas_call(mixer_kernel, out_shape=shape((n_lat, own_cols), BF16), in...  59.3 us
    unnamed x1, local copies, waits for them, and re-layouts  1.87 us

profile of v3, /device:TPU:1, one launch (start us, length us, event | category | flops | bytes accessed | tf_op | source)
XLA Modules:
  0.0 61.1 jit_solution(2389100744714880994)
XLA Ops:
  0.0 59.3 %mixer.1 = bf16[512,512]{1,0:T(8,128)(2,1)} custom-call(bf16[256]{0:T(256)(128)(2,1)} %cond_hbm.1, bf16[256]{0:T(256)(128)(2,1)} %cctx_hbm.1, bf16[256,512]{1,0:T(8,128)(2,1)} %shift_hbm.1, bf16[256,512]{1,0:T(8,128)(2,1)} %scale_hbm.1, bf16[256,512]{1,0:T(8,128)(2,1)} %gate_hbm.1, f32[1,4096]{1,0:T(1,128)} %bitcast.10, bf16[32,4096]{1,0:T(8,128)(2,1)} %bitcast.8, ...), custom_call_target="tpu_custom_call" | custom-call | tf_op jit(solution)/shard_map/mixer/pallas_call | solution.py:590
  59.3 1.9 %copy.20 = bf16[512,512]{1,0:T(8,128)(2,1)} copy(bf16[512,512]{1,0:T(8,128)(2,1)} %mixer.1) | data formatting | bytes 1048576

commit v4 on v3

--- a/solution.py
+++ b/solution.py
@@ -12,7 +12,7 @@
 F32 = jnp.float32
 BF16 = jnp.bfloat16
 TILE = 128
-VMEM_LIMIT = 67043328
+VMEM_LIMIT = 63_000_000
 MESH = pl.DeviceIdType.MESH
 LEVELS = (1, 2, 3, 4, 5, 6)
 
@@ -68,9 +68,11 @@
     bwd = logd
     s = 1
     while s < n_lat:
-        fwd = fwd + jnp.where(pos >= s, pltpu.roll(fwd, s, 1), 0.0)
-        bwd = bwd + jnp.where(pos + s < size, pltpu.roll(bwd, width - s, 1), 0.0)
-        s *= 2
+        ahead = [jnp.where(pos >= m * s, pltpu.roll(fwd, m * s, 1), 0.0) for m in range(1, 8)]
+        after = [jnp.where(pos + m * s < size, pltpu.roll(bwd, width - m * s, 1), 0.0) for m in range(1, 8)]
+        fwd = fwd + (((ahead[0] + ahead[1]) + (ahead[2] + ahead[3])) + ((ahead[4] + ahead[5]) + ahead[6]))
+        bwd = bwd + (((after[0] + after[1]) + (after[2] + after[3])) + ((after[4] + after[5]) + after[6]))
+        s *= 8
     g = jnp.where(row < 2, fwd, bwd)
     g = jnp.where(valid, g, 0.0)
     whole_lat = jnp.sum(jnp.where(is_ctx, 0.0, logd), axis=1, keepdims=True)
@@ -110,6 +112,12 @@
 RATE, G, LATE, EG, KINV = 0, 8, 16, 24, 32
 
 
+HANDS = (
+    "u0", "u1", "u2", "u3", "d0", "d1", "d2", "d3", "mA", "mB", "ru0", "ru1", "rd2", "rd3",
+    "mdA", "mdB", "muA", "muB", "ma0", "ma1", "ma2", "ma3",
+)
+
+
 def remote(src, dst, send_sem, recv_sem, axis, peer):
     return pltpu.make_async_remote_copy(
         src_ref=src, dst_ref=dst, send_sem=send_sem, recv_sem=recv_sem, device_id={axis: peer}, device_id_type=MESH
@@ -128,17 +136,13 @@
 
 def inverses(ad_ref, t_ref, base, count):
     xor = iota2((TILE, TILE), 0) ^ iota2((TILE, TILE), 1)
-    eye = jnp.where(xor == 0, 1.0, 0.0)
-    ts = []
-    for n in range(count):
-        a = ad_ref[base + n].astype(F32)
-        ts.append((eye - jnp.where(xor == 1, a, 0.0)).astype(BF16))
+    eye = jnp.where(xor == 0, 1.0, 0.0).astype(BF16)
+    near = jnp.where(xor == 1, 1.0, 0.0).astype(BF16)
+    ts = [eye - ad_ref[base + n] * near for n in range(count)]
     for level in LEVELS:
-        xs = []
-        for n in range(count):
-            off = jnp.where((xor >> level) == 1, ad_ref[base + n].astype(F32), 0.0).astype(BF16)
-            xs.append(mm(ts[n], off).astype(BF16))
-        ts = [(t.astype(F32) - mm(x, t)).astype(BF16) for x, t in zip(xs, ts)]
+        keep = jnp.where((xor >> level) == 1, 1.0, 0.0).astype(BF16)
+        xs = [mm(ts[n], ad_ref[base + n] * keep).astype(BF16) for n in range(count)]
+        ts = [t - mm(x, t).astype(BF16) for x, t in zip(xs, ts)]
     for n in range(count):
         t_ref[base + n] = ts[n]
 
@@ -148,7 +152,7 @@
     out_ref,
     rows_ref, cols_ref, gk_ref, qk_ref, dm_ref, ad_ref, t_ref, ao_ref, p_ref, x_ref, xl_ref, o1_ref, q2_ref,
     lat_map, ctx_map, lat_all, ctx_all, prefix_ref, lat_total, ctx_total, lat_totals, ctx_totals,
-    start_ref, mine_ref, ho_ref, send_sem, recv_sem, ho_send, ho_recv,
+    start_ref, mine_ref, ho_ref, acc_out, send_sem, recv_sem, ho_send, ho_recv,
 ):
     n_lat = q_ref.shape[0]
     n_ctx = k_ref.shape[0] - n_lat
@@ -221,19 +225,21 @@
         everyone[z_at] = total[...]
         return copies
 
+    krows = []
     for h in range(2):
-        krow = rows_ref[KINV + h : KINV + h + 1, 0:n_lat]
-        gk_ref[h] = mm_nt(kcols(h), kcols(h)) * kinv[h][0:n_lat] * krow
+        krows.append(jnp.log(rows_ref[KINV + h : KINV + h + 1, 0:n_lat]))
+        gk_ref[h] = mm_nt(kcols(h), kcols(h))
     for c in range(4):
         d, h = c // 2, c % 2
         for i in range(blocks):
-            ri = cols_ref[i * TILE : (i + 1) * TILE, RATE + c : RATE + c + 1]
+            ri = cols_ref[i * TILE : (i + 1) * TILE, RATE + c : RATE + c + 1] * kinv[h][i * TILE : (i + 1) * TILE]
             gi = cols_ref[i * TILE : (i + 1) * TILE, G + c : G + c + 1]
             for j in range(blocks):
                 if (d == 0 and j > i) or (d == 1 and j < i):
                     continue
                 at = (slice(i * TILE, (i + 1) * TILE), slice(j * TILE, (j + 1) * TILE))
-                sp = gi - rows_ref[G + c : G + c + 1, j * TILE : (j + 1) * TILE]
+                cj = slice(j * TILE, (j + 1) * TILE)
+                sp = gi - (rows_ref[G + c : G + c + 1, cj] - krows[h][:, cj])
                 if i == j:
                     keep = (ii >= jj) if d == 0 else (ii <= jj)
                     dm = jnp.where(keep, jnp.exp(jnp.where(keep, sp, 0.0)), 0.0)
@@ -316,7 +322,7 @@
         qh = q_ref[0:n_lat, h * TILE : (h + 1) * TILE]
         qinv = inv_norm(qh) * (HEAD_DIM**-0.5)
         qinvs.append(qinv)
-        qk_ref[h] = mm_nt(qh, kcols(h)) * qinv * rows_ref[KINV + h : KINV + h + 1, 0:n_lat]
+        qk_ref[h] = mm_nt(qh, kcols(h)) * qinv
     for c in range(4):
         d, h = c // 2, c % 2
         for i in range(blocks):
@@ -341,13 +347,13 @@
 
     for copy in lat_rows:
         copy.wait()
-    total = lat_all[place(0, 4)].astype(F32)
-    for n in range(1, 4):
-        at = place(n, 4)
-        prefix_ref[at] = total
-        total = then(lat_all[at], total)
-    lat_total[...] = total.astype(BF16)
+    low = lat_all[place(0, 4)].astype(F32)
+    pair = then(lat_all[place(1, 4)], low)
+    lat_total[...] = then(then(lat_all[place(3, 4)], lat_all[place(2, 4)].astype(F32)), pair).astype(BF16)
     lat_columns = to_column(9, lat_total, lat_totals)
+    prefix_ref[place(1, 4)] = low
+    prefix_ref[place(2, 4)] = pair
+    prefix_ref[place(3, 4)] = then(lat_all[place(2, 4)], pair)
     for copy in ctx_columns:
         copy.wait()
     state = None
@@ -371,68 +377,87 @@
     for copy in starts:
         copy.wait()
 
-    half = n_lat // 2
-    A, B = slice(0, half), slice(half, n_lat)
+    quarter = n_lat // 4
+    Q = [slice(n * quarter, (n + 1) * quarter) for n in range(4)]
+    A, B = slice(0, n_lat // 2), slice(n_lat // 2, n_lat)
+    both_s = [jnp.concatenate([mine_ref[h], mine_ref[2 + h]], axis=0) for h in range(2)]
 
     def finish(r):
         for h in range(2):
-            both_s = jnp.concatenate([mine_ref[h], mine_ref[2 + h]], axis=0)
-            y = o1_ref[h, r, :] + jnp.dot(q2_ref[h, r, :], both_s, preferred_element_type=F32)
+            y = o1_ref[h, r, :] + jnp.dot(q2_ref[h, r, :], both_s[h], preferred_element_type=F32)
             y = y * lax.rsqrt(jnp.mean(y * y, axis=-1, keepdims=True) + EPS) * gain_ref[...]
             ho_ref[t_at, r, h * TILE : (h + 1) * TILE] = y.astype(BF16)
 
-    def hand(n, block, r, peer):
-        copy = remote(ho_ref.at[block, r], ho_ref.at[block, r], ho_send.at[n], ho_recv.at[n], "tp", peer)
-        copy.start()
-        return copy
-
-    hands = {}
-    finish(A)
-    hands[0] = hand(0, t_at, A, up)
-    hands[4] = hand(4, t_at, A, mate)
-    finish(B)
-    hands[3] = hand(3, t_at, B, down)
-    hands[1] = hand(1, t_at, B, up)
-    hands[2] = hand(2, t_at, A, down)
-    hands[5] = hand(5, t_at, B, mate)
-    depth = 2 * TILE
-
-    def add(block):
-        w = ow_ref[pl.ds(pl.multiple_of(block * depth, depth), depth), :]
-        return jnp.dot(ho_ref[block], w, preferred_element_type=F32)
-
-    hands[0].wait_recv()
-    hands[6] = hand(6, down, A, up)
-    hands[8] = hand(8, down, A, mate)
-    hands[3].wait_recv()
-    hands[7] = hand(7, up, B, down)
-    hands[11] = hand(11, up, B, mate)
-    hands[4].wait_recv()
-    hands[5].wait_recv()
-    acc = add(t_at) + add(mate)
-    hands[1].wait_recv()
-    hands[9] = hand(9, down, B, mate)
-    hands[2].wait_recv()
-    hands[10] = hand(10, up, A, mate)
-    acc = acc + add(down) + add(up)
-    hands[6].wait_recv()
-    hands[12] = hand(12, across, A, mate)
-    hands[7].wait_recv()
-    hands[13] = hand(13, across, B, mate)
-    for n in range(8, 12):
-        hands[n].wait_recv()
-
     def other(block):
         return block + 1 - 2 * core
 
-    acc = acc + add(other(down)) + add(other(up)) + add(across)
-    hands[12].wait_recv()
-    hands[13].wait_recv()
-    acc = acc + add(other(across))
-    own = lat_ref[:, pl.ds(pl.multiple_of(t_at * own_cols, own_cols), own_cols)]
-    out_ref[...] = (own.astype(F32) + gate_row_ref[...] * acc).astype(BF16)
-    for n in range(14):
-        hands[n].wait_send()
+    hands = {}
+
+    def hand(name, block, r, peer):
+        n = HANDS.index(name)
+        hands[name] = remote(ho_ref.at[block, r], ho_ref.at[block, r], ho_send.at[n], ho_recv.at[n], "tp", peer)
+        hands[name].start()
+
+    def got(*names):
+        for name in names:
+            hands[name].wait_recv()
+
+    depth = 2 * TILE
+
+    def add(block, r=slice(None)):
+        w = ow_ref[pl.ds(pl.multiple_of(block * depth, depth), depth), :]
+        return jnp.dot(ho_ref[block, r], w, preferred_element_type=F32)
+
+    finish(Q[0])
+    hand("u0", t_at, Q[0], up)
+    finish(Q[3])
+    hand("d3", t_at, Q[3], down)
+    finish(Q[1])
+    hand("u1", t_at, Q[1], up)
+    hand("mA", t_at, A, mate)
+    finish(Q[2])
+    hand("d2", t_at, Q[2], down)
+    hand("u2", t_at, Q[2], up)
+    hand("u3", t_at, Q[3], up)
+    hand("d1", t_at, Q[1], down)
+    hand("d0", t_at, Q[0], down)
+    hand("mB", t_at, B, mate)
+    acc_out[...] = add(t_at)
+    got("mA", "mB")
+    acc_out[...] += add(mate)
+    got("u0")
+    hand("ru0", down, Q[0], up)
+    got("d3")
+    hand("rd3", up, Q[3], down)
+    got("u1")
+    hand("ru1", down, Q[1], up)
+    hand("mdA", down, A, mate)
+    got("d2")
+    hand("rd2", up, Q[2], down)
+    hand("muB", up, B, mate)
+    got("u2", "u3")
+    hand("mdB", down, B, mate)
+    got("d1", "d0")
+    hand("muA", up, A, mate)
+    acc_out[...] += add(down) + add(up)
+    got("ru0")
+    hand("ma0", across, Q[0], mate)
+    got("rd3")
+    hand("ma3", across, Q[3], mate)
+    got("mdA", "mdB", "muA", "muB")
+    acc_out[...] += add(other(down)) + add(other(up))
+    got("ru1")
+    hand("ma1", across, Q[1], mate)
+    got("rd2")
+    hand("ma2", across, Q[2], mate)
+    acc_out[...] += add(across)
+    gate = gate_row_ref[...]
+    own = pl.ds(pl.multiple_of(t_at * own_cols, own_cols), own_cols)
+    got("ma0", "ma3", "ma1", "ma2")
+    total = acc_out[...] + add(other(across))
+    out_ref[...] = (lat_ref[:, own].astype(F32) + gate * total).astype(BF16)
+    for name in HANDS:
+        hands[name].wait_send()
 
 
 def mixer_kernel(
@@ -470,7 +495,7 @@
             )
         )
     ]
-    for load in loads:
+    for load in loads[:5]:
         load.start()
     n_lat, n_ctx = lat_ref.shape[0], ctx_ref.shape[0]
     n_all = n_lat + n_ctx
@@ -479,6 +504,8 @@
     part_ref[...] = jnp.zeros_like(part_ref)
     for load in loads[:5]:
         load.wait()
+    for load in loads[5:7]:
+        load.start()
     u = jnp.concatenate(
         [cond_ref[...].astype(F32).reshape(1, -1), cctx_ref[...].astype(F32).reshape(1, -1)], axis=0
     )
@@ -494,6 +521,8 @@
         copy.start()
     for load in loads[5:7]:
         load.wait()
+    for load in loads[7:]:
+        load.start()
 
     def norms(src_ref, base):
         def step(i, carry):
@@ -589,7 +618,7 @@
     small = write_bias.shape
     return pl.pallas_call(
         mixer_kernel,
-        out_shape=shape((n_lat, own_cols), BF16),
+        out_shape=pltpu.VMEM((n_lat, own_cols), BF16),
         in_specs=[hb] * 18,
         out_specs=vm,
         scratch_shapes=[
@@ -616,9 +645,9 @@
             pltpu.VMEM((4, *one_map), F32), pltpu.VMEM(one_map, BF16), pltpu.VMEM(one_map, BF16),
             pltpu.VMEM((4, *one_map), BF16), pltpu.VMEM((4, *one_map), BF16),
             pltpu.VMEM((4, TILE, TILE), BF16), pltpu.VMEM((4, TILE, TILE), BF16),
-            pltpu.VMEM((8, n_lat, pair), BF16),
+            pltpu.VMEM((8, n_lat, pair), BF16), pltpu.VMEM((n_lat, own_cols), F32),
             pltpu.SemaphoreType.DMA((15,)), pltpu.SemaphoreType.DMA((15,)),
-            pltpu.SemaphoreType.DMA((14,)), pltpu.SemaphoreType.DMA((14,)),
+            pltpu.SemaphoreType.DMA((len(HANDS),)), pltpu.SemaphoreType.DMA((len(HANDS),)),
         ],
         compiler_params=pltpu.CompilerParams(
             collective_id=0, has_side_effects=True, vmem_limit_bytes=VMEM_LIMIT

time: 61.3 us -> 58.4 us (0.953)
  Pallas kernels: 59.3 us -> 57.5 us
  local copies, waits for them, and re-layouts: 1.87 us -> 0.8 us
    pallas_call x1, Pallas kernels: 59.3 us -> 57.5 us  [body(): pl.pallas_call(mixer_kernel, out_shape=pltpu.VMEM((n_lat, own_cols), BF16...]
    unnamed x1, local copies, waits for them, and re-layouts: 1.87 us -> 0.8 us
where the time goes in v4:
time: 58.4 us; the launch traced here: 58.3 us
  Pallas kernels  57.5 us (98%)
  local copies, waits for them, and re-layouts  0.8 us (1%)
    pallas_call x1, Pallas kernels, body(): pl.pallas_call(mixer_kernel, out_shape=pltpu.VMEM((n_lat, own_cols), BF16...  57.5 us

profile of v4, /device:TPU:1, one launch (start us, length us, event | category | flops | bytes accessed | tf_op | source)
XLA Modules:
  0.0 58.3 jit_solution(17370581107577879954)
XLA Ops:
  0.0 57.5 %mixer.1 = bf16[512,512]{1,0:T(8,128)(2,1)S(1)} custom-call(bf16[256]{0:T(256)(128)(2,1)} %cond_hbm.1, bf16[256]{0:T(256)(128)(2,1)} %cctx_hbm.1, bf16[256,512]{1,0:T(8,128)(2,1)} %shift_hbm.1, bf16[256,512]{1,0:T(8,128)(2,1)} %scale_hbm.1, bf16[256,512]{1,0:T(8,128)(2,1)} %gate_hbm.1, f32[1,4096]{1,0:T(1,128)} %bitcast.10, bf16[32,4096]{1,0:T(8,128)(2,1)} %bitcast.8, ...), custom_call_target="tpu_custom_call" | custom-call | tf_op jit(solution)/shard_map/mixer/pallas_call | solution.py:619
  57.5 0.8 %copy.20 = bf16[512,512]{1,0:T(8,128)(2,1)} copy(bf16[512,512]{1,0:T(8,128)(2,1)S(1)} %mixer.1) | data formatting | bytes 1048576

commit v5 on v4

--- a/solution.py
+++ b/solution.py
@@ -252,7 +252,7 @@
                     ao_ref[(c, *at)] = a.astype(BF16)
                 dm_ref[(c, *at)] = dm
 
-    inverses(ad_ref, t_ref, 0, ad_ref.shape[0])
+    inverses(ad_ref, t_ref, 4 * blocks, 2)
     for h in range(2):
         ci = kinv[h][n_lat:]
         cr = slice(n_lat, n_lat + TILE)
@@ -270,6 +270,8 @@
             ctx_map[c] = jnp.concatenate([diag - m[:, TILE:], m[:, :TILE]], axis=1).astype(BF16)
 
     ctx_rows = to_row(0, ctx_map, ctx_all)
+
+    inverses(ad_ref, t_ref, 0, 4 * blocks)
 
     backwards = x_at >= 2
 
@@ -309,14 +311,6 @@
         lat_map[c] = jnp.concatenate([diag - m[:, TILE:], m[:, :TILE]], axis=1).astype(BF16)
     lat_rows = to_row(6, lat_map, lat_all)
 
-    for copy in ctx_rows:
-        copy.wait()
-    total = ctx_all[place(0, 4)].astype(F32)
-    for n in range(1, 4):
-        total = then(ctx_all[place(n, 4)], total)
-    ctx_total[...] = total.astype(BF16)
-    ctx_columns = to_column(3, ctx_total, ctx_totals)
-
     qinvs = []
     for h in range(2):
         qh = q_ref[0:n_lat, h * TILE : (h + 1) * TILE]
@@ -344,6 +338,14 @@
                     o1.append(ow[:, :TILE])
                 else:
                     o1_ref[h, r, :] = o1[i] + ow[:, :TILE]
+
+    for copy in ctx_rows:
+        copy.wait()
+    total = ctx_all[place(0, 4)].astype(F32)
+    for n in range(1, 4):
+        total = then(ctx_all[place(n, 4)], total)
+    ctx_total[...] = total.astype(BF16)
+    ctx_columns = to_column(3, ctx_total, ctx_totals)
 
     for copy in lat_rows:
         copy.wait()
@@ -453,9 +455,13 @@
     acc_out[...] += add(across)
     gate = gate_row_ref[...]
     own = pl.ds(pl.multiple_of(t_at * own_cols, own_cols), own_cols)
-    got("ma0", "ma3", "ma1", "ma2")
-    total = acc_out[...] + add(other(across))
-    out_ref[...] = (lat_ref[:, own].astype(F32) + gate * total).astype(BF16)
+    got("ma0", "ma3", "ma1")
+    for r in (A, Q[3]):
+        total = acc_out[r, :] + add(other(across), r)
+        out_ref[r, :] = (lat_ref[r, own].astype(F32) + gate * total).astype(BF16)
+    got("ma2")
+    total = acc_out[Q[2], :] + add(other(across), Q[2])
+    out_ref[Q[2], :] = (lat_ref[Q[2], own].astype(F32) + gate * total).astype(BF16)
     for name in HANDS:
         hands[name].wait_send()
 

time: 58.4 us -> 56.2 us (0.962)
  Pallas kernels: 57.5 us -> 55.3 us
    pallas_call x1, Pallas kernels: 57.5 us -> 55.3 us  [body(): pl.pallas_call(mixer_kernel, out_shape=pltpu.VMEM((n_lat, own_cols), BF16...]
where the time goes in v5:
time: 56.2 us; the launch traced here: 56.1 us
  Pallas kernels  55.3 us (98%)
  local copies, waits for them, and re-layouts  0.8 us (1%)
    pallas_call x1, Pallas kernels, body(): pl.pallas_call(mixer_kernel, out_shape=pltpu.VMEM((n_lat, own_cols), BF16...  55.3 us

profile of v5, /device:TPU:1, one launch (start us, length us, event | category | flops | bytes accessed | tf_op | source)
XLA Modules:
  0.0 56.1 jit_solution(17316829052537757376)
XLA Ops:
  0.0 55.3 %mixer.1 = bf16[512,512]{1,0:T(8,128)(2,1)S(1)} custom-call(bf16[256]{0:T(256)(128)(2,1)} %cond_hbm.1, bf16[256]{0:T(256)(128)(2,1)} %cctx_hbm.1, bf16[256,512]{1,0:T(8,128)(2,1)} %shift_hbm.1, bf16[256,512]{1,0:T(8,128)(2,1)} %scale_hbm.1, bf16[256,512]{1,0:T(8,128)(2,1)} %gate_hbm.1, f32[1,4096]{1,0:T(1,128)} %bitcast.10, bf16[32,4096]{1,0:T(8,128)(2,1)} %bitcast.8, ...), custom_call_target="tpu_custom_call" | custom-call | tf_op jit(solution)/shard_map/mixer/pallas_call | solution.py:625
  55.3 0.8 %copy.20 = bf16[512,512]{1,0:T(8,128)(2,1)} copy(bf16[512,512]{1,0:T(8,128)(2,1)S(1)} %mixer.1) | data formatting | bytes 1048576

commit v6 on v5

--- a/solution.py
+++ b/solution.py
@@ -411,14 +411,14 @@
         return jnp.dot(ho_ref[block, r], w, preferred_element_type=F32)
 
     finish(Q[0])
+    finish(Q[3])
     hand("u0", t_at, Q[0], up)
-    finish(Q[3])
     hand("d3", t_at, Q[3], down)
     finish(Q[1])
+    finish(Q[2])
     hand("u1", t_at, Q[1], up)
+    hand("d2", t_at, Q[2], down)
     hand("mA", t_at, A, mate)
-    finish(Q[2])
-    hand("d2", t_at, Q[2], down)
     hand("u2", t_at, Q[2], up)
     hand("u3", t_at, Q[3], up)
     hand("d1", t_at, Q[1], down)
@@ -581,10 +581,10 @@
             ]
             piece_ref[slot, base : base + count, :] = jnp.concatenate(y, axis=1).astype(BF16)
         m = piece_ref[slot]
+        pre_acc[0:n_all, 0:64] += mm_nt(m, wg_ref[:, cols])
         acc_ref[0] += jnp.dot(m, w_ref[0, cols, :], preferred_element_type=F32)
         acc_ref[1] += jnp.dot(m, w_ref[1, cols, :], preferred_element_type=F32)
         acc_ref[2, 0:n_lat] += jnp.dot(m[0:n_lat], w_ref[2, cols, :], preferred_element_type=F32)
-        pre_acc[0:n_all, 0:64] += mm_nt(m, wg_ref[:, cols])
 
     piece(0, t)
     for n, block in enumerate(sources):

time: 56.2 us -> 55.7 us (level)
  no operation moved by 1% of the time
where the time goes in v6:
time: 55.7 us; the launch traced here: 55.6 us
  Pallas kernels  54.8 us (98%)
  local copies, waits for them, and re-layouts  0.8 us (1%)
    pallas_call x1, Pallas kernels, body(): pl.pallas_call(mixer_kernel, out_shape=pltpu.VMEM((n_lat, own_cols), BF16...  54.8 us

profile of v6, /device:TPU:1, one launch (start us, length us, event | category | flops | bytes accessed | tf_op | source)
XLA Modules:
  0.0 55.6 jit_solution(14723877783359227252)
XLA Ops:
  0.0 54.8 %mixer.1 = bf16[512,512]{1,0:T(8,128)(2,1)S(1)} custom-call(bf16[256]{0:T(256)(128)(2,1)} %cond_hbm.1, bf16[256]{0:T(256)(128)(2,1)} %cctx_hbm.1, bf16[256,512]{1,0:T(8,128)(2,1)} %shift_hbm.1, bf16[256,512]{1,0:T(8,128)(2,1)} %scale_hbm.1, bf16[256,512]{1,0:T(8,128)(2,1)} %gate_hbm.1, f32[1,4096]{1,0:T(1,128)} %bitcast.10, bf16[32,4096]{1,0:T(8,128)(2,1)} %bitcast.8, ...), custom_call_target="tpu_custom_call" | custom-call | tf_op jit(solution)/shard_map/mixer/pallas_call | solution.py:625
  54.8 0.8 %copy.20 = bf16[512,512]{1,0:T(8,128)(2,1)} copy(bf16[512,512]{1,0:T(8,128)(2,1)S(1)} %mixer.1) | data formatting | bytes 1048576
